TPU v7x, 32 devices: a whole 2x2x4 slice. The times are simulated.
32 devices in a mesh: ep: 4 (over y, x), tp: 8 (over z, core).
Axes of the slice: x: 2, y: 2, z: 4, core: 2. Of those that a mesh axis runs over, the one named last changes fastest.
Arguments:
- query_preactivation: bfloat16 [8192, 2048], P('ep', 'tp'), may hold values from -6 to 6
- forget_preactivation: bfloat16 [8192, 2048], P('ep', 'tp'), may hold values from -6 to 6
- value_input_rows: bfloat16 [8192, 1024], P('ep', 'tp'), may hold values from -8 to 8
- output_gate_preactivation: bfloat16 [8192, 1024], P('ep', 'tp'), may hold values from -6 to 6
- forget_floor_gap: float32 [2048], P('tp'), may hold values from 0 to 0.2, as said below
- extra_log_forget: float32 [8192, 16], P('ep', 'tp'), may hold values from -2 to 0
- head_output_gain: float32 [1024], P('tp'), may hold values from 0.1 to 1.9
- mixer_output_weight: bfloat16 [1024, 2048], P(None, 'tp'), may hold values from -0.1875 to 0.1875
- second_batch_tokens: bfloat16 [2048, 2048], P('ep'), may hold values from -6 to 6
- feedforward_norm_gain: float32 [2048], replicated, may hold values from 0.1 to 1.9
- chosen_expert_index: int32 [2048, 2], P('ep'), may hold values from 0 to 3, all different within a row; in each aligned block of 64 rows (0 to 63, 64 to 127, ...) at most 40 rows name the same one
- chosen_expert_weight: float32 [2048, 2], P('ep'), may hold values from 0.1 to 1
- expert_gate_weight: bfloat16 [4, 2048, 7168], P('ep', None, 'tp'), may hold values from -0.125 to 0.125
- expert_up_weight: bfloat16 [4, 2048, 7168], P('ep', None, 'tp'), may hold values from -0.125 to 0.125
- expert_down_weight: bfloat16 [4, 7168, 2048], P('ep', 'tp'), may hold values from -0.0625 to 0.0625
Outputs:
- mixer_output_first: bfloat16 [8192, 2048], P('ep', 'tp')
- moe_out: bfloat16 [2048, 2048], P(('ep', 'tp'))
Inputs may be any that keep to these rules, and one draw needn't show every extreme that they name: `chosen_expert_index`: each row names 2 different experts. In each aligned block of 64 rows (the rows of one device's share) no expert is named by more than 40 rows, and in every draw some expert is named by exactly 40 rows of some block. `forget_floor_gap`: every entry is positive.
All inputs are finite; a program needn't handle non-finite values.
Results may differ from a plain program's by a relative error of at most 0.019.
Values may be sent and summed in bfloat16 or wider, within the bound.
A program may use at most 128 MiB of HBM per device.

v0:
```python
import functools

import jax
import jax.numpy as jnp
from jax import lax
from jax.experimental import pallas as pl
from jax.experimental.pallas import tpu as pltpu
from jax.sharding import PartitionSpec as P

KEY_DIM = 128
VAL_DIM = 64
BLOCK_POSITIONS = 64
TOPK = 2


epsilon = 1e-06


CHUNK = 256
NT = (((1,), (1,)), ((), ()))
TN = (((0,), (0,)), ((), ()))


def local_kernel(heads, q_ref, f_ref, v_ref, gap_ref, extra_ref, rec_ref, qdec_ref, carry_ref, state, base):
    step = pl.program_id(0)

    @pl.when(step == 0)
    def _():
        state[...] = jnp.zeros_like(state)
        base[...] = jnp.zeros_like(base)

    rows, vals = v_ref.shape
    q = q_ref[...].astype(jnp.float32)
    q = q / (1.0 + jnp.exp(-q))
    key = gap_ref[...] / (1.0 + jnp.exp(f_ref[...].astype(jnp.float32)))
    extra = extra_ref[...]
    log_forget = jnp.log(1.0 - key) + jnp.concatenate(
        [jnp.broadcast_to(extra[:, h : h + 1], (rows, KEY_DIM)) for h in range(heads)], axis=1
    )
    at = lax.broadcasted_iota(jnp.int32, (rows, rows), 0)
    of = lax.broadcasted_iota(jnp.int32, (rows, rows), 1)
    lower = jnp.where((at >= of) & (at // BLOCK_POSITIONS == of // BLOCK_POSITIONS), 1.0, 0.0)
    lower = lower.astype(jnp.bfloat16)
    high = log_forget.astype(jnp.bfloat16)
    low = (log_forget - high.astype(jnp.float32)).astype(jnp.bfloat16)
    cumulative = jnp.dot(lower, high, preferred_element_type=jnp.float32) + jnp.dot(
        lower, low, preferred_element_type=jnp.float32
    )
    causal = lax.broadcasted_iota(
        jnp.int32, (BLOCK_POSITIONS, BLOCK_POSITIONS), 0
    ) >= lax.broadcasted_iota(jnp.int32, (BLOCK_POSITIONS, BLOCK_POSITIONS), 1)
    lane_head = lax.broadcasted_iota(jnp.int32, (BLOCK_POSITIONS, vals), 1) // VAL_DIM
    held = [state[h] for h in range(heads)]
    before = base[...]
    half = BLOCK_POSITIONS // 2
    for b in range(rows // BLOCK_POSITIONS):
        part = slice(b * BLOCK_POSITIONS, (b + 1) * BLOCK_POSITIONS)
        cum = cumulative[part]
        mid, last = cum[half - 1 : half], cum[BLOCK_POSITIONS - 1 :]
        q_part = q[part]
        q_mid = (q_part * jnp.exp(cum - mid)).astype(jnp.bfloat16)
        k_mid = (key[part] * jnp.exp(mid - cum)).astype(jnp.bfloat16)
        qdec_ref[part, :] = (q_part * jnp.exp(cum + before)).astype(jnp.bfloat16)
        decay_mid, decay_last, decay_rest = jnp.exp(mid), jnp.exp(last), jnp.exp(last - mid)
        before = before + last
        values = v_ref[part, :]
        out = jnp.zeros((BLOCK_POSITIONS, vals), jnp.float32)
        for h in range(heads):
            lanes = slice(h * KEY_DIM, (h + 1) * KEY_DIM)
            across = lax.dot_general(
                q_mid[:, lanes],
                (held[h] * decay_mid[:, lanes]).astype(jnp.bfloat16),
                NT,
                preferred_element_type=jnp.float32,
            )
            scores = lax.dot_general(
                q_mid[:, lanes], k_mid[:, lanes], NT, preferred_element_type=jnp.float32
            )
            scores = jnp.where(causal, scores, 0.0).astype(jnp.bfloat16)
            within = jnp.dot(scores, values, preferred_element_type=jnp.float32)
            out = jnp.where(lane_head == h, within + across, out)
            update = lax.dot_general(
                values, k_mid[:, lanes], TN, preferred_element_type=jnp.float32
            )
            held[h] = held[h] * decay_last[:, lanes] + update * decay_rest[:, lanes]
        rec_ref[part, :] = out
    for h in range(heads):
        state[h] = held[h]
    base[...] = before

    @pl.when(step == pl.num_programs(0) - 1)
    def _():
        own = [held[h][h * VAL_DIM : (h + 1) * VAL_DIM] for h in range(heads)]
        carry_ref[:VAL_DIM, :] = jnp.concatenate(own, axis=1).astype(jnp.bfloat16)
        total = jnp.exp(before)
        carry_ref[VAL_DIM:, :] = jnp.broadcast_to(total, (16, total.shape[1])).astype(jnp.bfloat16)


def local_recurrence(query, forget, values, gap, extra):
    length, keys = query.shape
    heads, vals = keys // KEY_DIM, values.shape[1]

    def chunk(width):
        return pl.BlockSpec((CHUNK, width), lambda i: (i, 0))

    return pl.pallas_call(
        functools.partial(local_kernel, heads),
        grid=(length // CHUNK,),
        in_specs=[
            chunk(keys),
            chunk(keys),
            chunk(vals),
            pl.BlockSpec((1, keys), lambda i: (0, 0)),
            chunk(heads),
        ],
        out_specs=[
            chunk(vals),
            chunk(keys),
            pl.BlockSpec((VAL_DIM + 16, keys), lambda i: (0, 0)),
        ],
        out_shape=[
            jax.ShapeDtypeStruct((length, vals), jnp.float32),
            jax.ShapeDtypeStruct((length, keys), jnp.bfloat16),
            jax.ShapeDtypeStruct((VAL_DIM + 16, keys), jnp.bfloat16),
        ],
        scratch_shapes=[
            pltpu.VMEM((heads, vals, KEY_DIM), jnp.float32),
            pltpu.VMEM((1, keys), jnp.float32),
        ],
        cost_estimate=pl.CostEstimate(
            flops=10_000_000_000, bytes_accessed=6_000_000, transcendentals=3_000_000
        ),
        name="local_recurrence",
    )(query, forget, values, gap.reshape(1, keys), extra)


def gate_kernel(heads, places, place_ref, rec_ref, qdec_ref, carry_ref, gain_ref, gate_ref, out_ref, held):
    rows, vals = rec_ref.shape

    @pl.when(pl.program_id(0) == 0)
    def _():
        place = place_ref[0]
        total = jnp.zeros((VAL_DIM, heads * KEY_DIM), jnp.float32)
        for i in range(places):
            decay = carry_ref[i, VAL_DIM:, :].astype(jnp.float32)[:1]
            joined = total * decay + carry_ref[i, :VAL_DIM, :].astype(jnp.float32)
            total = jnp.where(i < place, joined, total)
        lane_head = lax.broadcasted_iota(jnp.int32, total.shape, 1) // KEY_DIM
        for h in range(heads):
            held[h * VAL_DIM : (h + 1) * VAL_DIM, :] = jnp.where(lane_head == h, total, 0.0).astype(
                jnp.bfloat16
            )

    rec = rec_ref[...] + lax.dot_general(
        qdec_ref[...], held[...], NT, preferred_element_type=jnp.float32
    )
    at = lax.broadcasted_iota(jnp.int32, (vals, vals), 0) // VAL_DIM
    of = lax.broadcasted_iota(jnp.int32, (vals, vals), 1) // VAL_DIM
    average = jnp.where(at == of, 1.0 / VAL_DIM, 0.0).astype(jnp.bfloat16)
    square = rec * rec
    high = square.astype(jnp.bfloat16)
    low = (square - high.astype(jnp.float32)).astype(jnp.bfloat16)
    mean = jnp.dot(high, average, preferred_element_type=jnp.float32) + jnp.dot(
        low, average, preferred_element_type=jnp.float32
    )
    gate = gate_ref[...].astype(jnp.float32)
    gate = gate / (1.0 + jnp.exp(-gate))
    out_ref[...] = (rec * lax.rsqrt(mean + epsilon) * gain_ref[...] * gate).astype(jnp.bfloat16)


def gated_output(rec, qdec, carries, gain, gate):
    length, vals = rec.shape
    keys = qdec.shape[1]
    heads = keys // KEY_DIM
    rows = 2 * CHUNK

    def chunk(width):
        return pl.BlockSpec((rows, width), lambda i: (i, 0))

    return pl.pallas_call(
        functools.partial(gate_kernel, heads, carries.shape[0]),
        grid=(length // rows,),
        in_specs=[
            pl.BlockSpec(memory_space=pltpu.SMEM),
            chunk(vals),
            chunk(keys),
            pl.BlockSpec(carries.shape, lambda i: (0, 0, 0)),
            pl.BlockSpec((1, vals), lambda i: (0, 0)),
            chunk(vals),
        ],
        out_specs=chunk(vals),
        out_shape=jax.ShapeDtypeStruct((length, vals), jnp.bfloat16),
        scratch_shapes=[pltpu.VMEM((vals, keys), jnp.bfloat16)],
        cost_estimate=pl.CostEstimate(
            flops=2_000_000_000, bytes_accessed=3_000_000, transcendentals=1_000_000
        ),
        name="gated_output",
    )(lax.axis_index("ep").reshape(1), rec, qdec, carries, gain.reshape(1, vals), gate)


def norm_rows(tokens, row_gain):
    tokens_float = tokens.astype(jnp.float32)
    factor = lax.rsqrt(jnp.mean(tokens_float * tokens_float, axis=-1, keepdims=True) + epsilon)
    return (tokens_float * factor * row_gain).astype(jnp.bfloat16)


def slot_positions(blocks, experts_all):
    flattened = blocks.reshape(blocks.shape[0], -1)
    onehot = (flattened[..., None] == jnp.arange(experts_all, dtype=jnp.int32)).astype(jnp.int32)
    earlier = jnp.cumsum(onehot, axis=1) - onehot
    return jnp.sum(earlier * onehot, axis=-1).reshape(blocks.shape)


def fill_slots(rows_in, blocks, slot_ids, experts_all, capacity):
    groups = blocks.shape[0]
    sub_rows = blocks.shape[1]
    group_ids = jnp.arange(groups, dtype=jnp.int32)[:, None, None]
    target = (group_ids * experts_all + blocks) * capacity + slot_ids
    sources = jnp.broadcast_to(
        jnp.arange(sub_rows, dtype=jnp.int32)[None, :, None] + group_ids * sub_rows, blocks.shape
    )
    lookup = (
        jnp.full((groups * experts_all * capacity,), -1, jnp.int32)
        .at[target.reshape(-1)]
        .set(sources.reshape(-1))
    )
    gathered = rows_in.reshape(groups * sub_rows, -1)[jnp.maximum(lookup, 0)]
    filled = jnp.where((lookup >= 0)[:, None], gathered, jnp.zeros((), gathered.dtype))
    return filled.reshape(groups, experts_all, capacity, -1)


def on_device(
    query_preactivation,
    forget_preactivation,
    value_input_rows,
    output_gate_preactivation,
    forget_floor_gap,
    extra_log_forget,
    head_output_gain,
    mixer_output_weight,
    second_batch_tokens,
    feedforward_norm_gain,
    chosen_expert_index,
    chosen_expert_weight,
    expert_gate_weight,
    expert_up_weight,
    expert_down_weight,
):
    local_experts = expert_gate_weight.shape[0]
    places = lax.axis_size("ep")
    experts_all = local_experts * places
    groups = lax.axis_size("tp")
    width = second_batch_tokens.shape[1]
    sub_rows = second_batch_tokens.shape[0] // groups
    capacity = max(2, sub_rows * TOPK * 5 // (4 * experts_all))
    place = lax.axis_index("ep")
    position = lax.axis_index("tp")
    pairs = groups // 2
    side = lax.rem(position, 2)

    all_routes = chosen_expert_index.reshape(pairs, 2, sub_rows, TOPK)
    routes = lax.dynamic_index_in_dim(all_routes, side, 1, False)
    all_tokens = second_batch_tokens.reshape(pairs, 2, sub_rows, width)
    tokens = lax.dynamic_index_in_dim(all_tokens, side, 1, False)
    slots = slot_positions(routes, experts_all)
    outgoing = fill_slots(
        norm_rows(tokens, feedforward_norm_gain), routes, slots, experts_all, capacity
    )
    outgoing, query_preactivation = lax.optimization_barrier((outgoing, query_preactivation))
    outgoing = outgoing.reshape(pairs, places, local_experts, capacity, width)
    arrived = []
    for step in range(places):
        block = lax.dynamic_index_in_dim(outgoing, place ^ step, 1, False)
        if step:
            block = lax.ppermute(block, "ep", [(i, i ^ step) for i in range(places)])
        arrived.append(block)
    partners = [(i, i ^ 1) for i in range(groups)]
    shape = (pairs, places, local_experts, capacity, width)
    others = [lax.ppermute(block, "tp", partners) for block in arrived]
    own_side = jnp.stack(arrived, axis=1)
    other_side = jnp.stack(others, axis=1)

    recurrent, query_decayed, carry = local_recurrence(
        query_preactivation,
        forget_preactivation,
        value_input_rows,
        forget_floor_gap,
        extra_log_forget,
    )
    carries = lax.all_gather(carry, "ep")
    mixed = gated_output(
        recurrent, query_decayed, carries, head_output_gain, output_gate_preactivation
    )
    mixed_all = lax.all_gather(mixed, "tp", axis=1, tiled=True)

    def experts(rows):
        gate_part = jnp.einsum(
            "tsecd,edf->tsecf", rows, expert_gate_weight, preferred_element_type=jnp.float32
        )
        up_part = jnp.einsum(
            "tsecd,edf->tsecf", rows, expert_up_weight, preferred_element_type=jnp.float32
        )
        hidden = (jax.nn.silu(gate_part) * up_part).astype(jnp.bfloat16)
        product = jnp.einsum(
            "tsecf,efd->tsecd", hidden, expert_down_weight, preferred_element_type=jnp.float32
        )
        return product.astype(jnp.bfloat16)

    other_side, mixed = lax.optimization_barrier((other_side, mixed))
    for_partner = experts(other_side)
    own_side, for_partner = lax.optimization_barrier((own_side, for_partner))
    from_partner = lax.ppermute(for_partner, "tp", partners)
    product = experts(own_side).astype(jnp.float32) + from_partner.astype(jnp.float32)
    product, mixed_all = lax.optimization_barrier((product.astype(jnp.bfloat16), mixed_all))
    to_return = lax.psum_scatter(
        product,
        "tp",
        scatter_dimension=0,
        tiled=True,
        axis_index_groups=[list(range(c, groups, 2)) for c in range(2)],
    )
    to_return = to_return.reshape(shape[1:])
    mixer_output_first = jnp.dot(
        mixed_all, mixer_output_weight, preferred_element_type=jnp.float32
    ).astype(jnp.bfloat16)
    returned = []
    for step in range(places):
        block = to_return[step]
        if step:
            block = lax.ppermute(block, "ep", [(i, i ^ step) for i in range(places)])
        returned.append(block)
    results = jnp.concatenate(returned, axis=0).reshape(experts_all * capacity, width)
    own_routes = lax.dynamic_index_in_dim(routes, position // 2, 0, False)
    own_slots = lax.dynamic_index_in_dim(slots, position // 2, 0, False)
    own_weights = lax.dynamic_slice_in_dim(chosen_expert_weight, position * sub_rows, sub_rows, 0)
    holder = (own_routes // local_experts) ^ place
    flat_index = (holder * local_experts + own_routes % local_experts) * capacity + own_slots
    combined = jnp.zeros((sub_rows, width), jnp.float32)
    for ranked in range(TOPK):
        combined = (
            combined
            + results[flat_index[:, ranked]].astype(jnp.float32)
            * own_weights[:, ranked : ranked + 1]
        )
    return (mixer_output_first, combined.astype(jnp.bfloat16))


def solution(mesh):
    placed = (
        P("ep", "tp"),
        P("ep", "tp"),
        P("ep", "tp"),
        P("ep", "tp"),
        P("tp"),
        P("ep", "tp"),
        P("tp"),
        P(None, "tp"),
        P("ep", None),
        P(),
        P("ep", None),
        P("ep", None),
        P("ep", None, "tp"),
        P("ep", None, "tp"),
        P("ep", "tp", None),
    )
    return jax.shard_map(
        on_device,
        mesh=mesh,
        in_specs=placed,
        out_specs=(P("ep", "tp"), P(("ep", "tp"), None)),
        check_vma=False,
    )
```

profile of v0, /device:TPU:0, one launch (start us, length us, event | category | flops | bytes accessed | tf_op | source)
XLA Modules:
  0.0 194.6 jit_solution(2632501884968382120)
XLA Ops:
  7.3 3.0 %bitcast_convert_fusion = f32[4,1,64,2048]{3,2,0,1:T(8,128)} fusion(bf16[4,2,64,2048]{3,2,1,0:T(8,128)(2,1)} %bitcast.217, s32[]{:T(128)S(6)} %select_n.69), kind=kLoop, calls=%fused_computation.50 | loop fusion | flops 524288 | bytes 3145732 | tf_op jit(solution)/shard_map/convert_element_type | solution.py:202
  12.3 2.4 %scatter_custom_fusion = s32[640]{0:T(1024)S(1)} fusion(s32[512]{0:T(512)S(1)} %bitcast.232, s32[512]{0:T(512)S(1)} %reshape.246, s32[]{:T(128)} %constant.113.clone.1), kind=kCustom, calls=%fused_computation.78 | custom fusion | bytes 2564 | tf_op jit(solution)/shard_map/scatter | solution.py:225
  15.0 1.8 fusion.40
  16.9 4.1 %gather_fusion = bf16[640,2048]{1,0:T(8,128)(2,1)} fusion(bf16[256,2048]{1,0:T(8,128)(2,1)S(1)} %fusion.40, s32[1024]{0:T(1024)S(1)} %pad_clamp_fusion.2), kind=kCustom, calls=%fused_computation | custom fusion | bytes 5245440 | tf_op jit(solution)/shard_map/gather | solution.py:227
  21.0 2.0 %copy_select_fusion = bf16[4,4,40,2048]{3,2,0,1:T(8,128)(2,1)S(1)} fusion(bf16[4,4,40,2048]{3,2,1,0:T(8,128)(2,1)} %bitcast.215, pred[4,4,40]{2,0,1:T(4,128)(4,1)S(1)} %copy.49), kind=kLoop, calls=%fused_computation.26 | loop fusion | flops 1310720 | bytes 5243520 | tf_op jit(solution)/shard_map/jit(_where)/select_n | solution.py:228
  24.3 15.7 %local_recurrence.1 = (f32[2048,128]{1,0:T(8,128)}, bf16[2048,256]{1,0:T(8,128)(2,1)}, bf16[80,256]{1,0:T(8,128)(2,1)}) custom-call(bf16[2048,256]{1,0:T(8,128)(2,1)} %q_ref, bf16[2048,256]{1,0:T(8,128)(2,1)} %f_ref.1, bf16[2048,128]{1,0:T(8,128)(2,1)} %v_ref.1, f32[1,256]{1,0:T(1,128)} %bitcast.233, f32[2048,2]{1,0:T(8,128)} %copy.54.extra_ref), custom_call_target="tpu_custom_call" | custom-call | flops 10000000000 | bytes 6000000 | tf_op jit(solution)/shard_map/local_recurrence/pallas_call | solution.py:106
  40.0 11.6 %all-gather = bf16[320,256]{1,0:T(8,128)(2,1)} all-gather(bf16[80,256]{1,0:T(8,128)(2,1)} %get-tuple-element.16), channel_id=2, replica_groups=mesh['ep'=4,'tp'=8] {'ep'}, dimensions={0}, use_global_device_ids=true | all-gather | bytes 204800 | tf_op jit(solution)/shard_map/all_gather | solution.py:290
  51.6 4.7 %gated_output.1 = bf16[2048,128]{1,0:T(8,128)(2,1)} custom-call(s32[1]{0:T(128)} %bitcast.16.place_ref, f32[2048,128]{1,0:T(8,128)} %get-tuple-element.14.rec_ref, bf16[2048,256]{1,0:T(8,128)(2,1)} %get-tuple-element.15.qdec_ref, bf16[4,80,256]{2,1,0:T(8,128)(2,1)} %bitcast.229, f32[1,128]{1,0:T(1,128)} %bitcast.234, bf16[2048,128]{1,0:T(8,128)(2,1)} %gate_ref.1), custom_call_target="tpu_custom_call" | custom-call | flops 2000000000 | bytes 3000000 | tf_op jit(solution)/shard_map/gated_output/pallas_call | solution.py:180
  57.4 1.4 collective-permute-start.1
  58.8 1.5 collective-permute-start.2
  60.3 14.1 %collective-permute-done = bf16[4,1,40,2048]{3,2,0,1:T(8,128)(2,1)S(1)} collective-permute-done((bf16[4,1,40,2048]{3,2,0,1:T(8,128)(2,1)S(1)}, bf16[4,1,40,2048]{3,2,0,1:T(8,128)(2,1)S(1)}, u32[]{:S(2)}, u32[]{:S(2)}) %collective-permute-start) | collective-permute-done | bytes 655392 | tf_op jit(solution)/shard_map/ppermute | solution.py:275
  74.4 11.5 %collective-permute-done.1 = bf16[4,1,40,2048]{3,2,0,1:T(8,128)(2,1)S(1)} collective-permute-done((bf16[4,1,40,2048]{3,2,0,1:T(8,128)(2,1)S(1)}, bf16[4,1,40,2048]{3,2,0,1:T(8,128)(2,1)S(1)}, u32[]{:S(2)}, u32[]{:S(2)}) %collective-permute-start.1) | collective-permute-done | bytes 655392 | tf_op jit(solution)/shard_map/ppermute | solution.py:275
  86.8 1.5 collective-permute-done.5
  89.7 1.5 copy-done.1
  92.3 4.3 %fusion.7 = f32[4,4,40,896]{3,2,1,0:T(8,128)} fusion(bf16[1,2048,896]{2,1,0:T(8,128)(2,1)S(1)} %copy-done.6, bf16[4,4,1,40,2048]{4,3,0,2,1:T(8,128)(2,1)S(1)} %pad_maximum_fusion.1), kind=kOutput, calls=%fused_computation.12 | convolution fusion | flops 2348810240 | bytes 8585216 | tf_op jit(solution)/shard_map/tsecd,edf->tsecf/dot_general | solution.py:297
  96.6 11.8 %fusion.22 = bf16[4,4,1,40,2048]{4,3,1,0,2:T(8,128)(2,1)} fusion(bf16[1,896,2048]{2,1,0:T(8,128)(2,1)} %param.29, bf16[1,2048,896]{2,1,0:T(8,128)(2,1)} %param.28, f32[4,4,40,896]{3,2,1,0:T(8,128)} %fusion.7, bf16[4,4,1,40,2048]{4,3,0,2,1:T(8,128)(2,1)} %copy-done.1), kind=kOutput, calls=%fused_computation.21 | convolution fusion | flops 4702371840 | bytes 14876672 | tf_op jit(solution)/shard_map/tsecf,efd->tsecd/dot_general | solution.py:304
  108.6 5.1 %fusion.5 = f32[4,4,40,896]{3,2,1,0:T(8,128)S(1)} fusion(bf16[1,2048,896]{2,1,0:T(8,128)(2,1)} %param.27, bf16[4,4,1,40,2048]{4,3,1,0,2:T(8,128)(2,1)S(1)} %pad_maximum_fusion), kind=kOutput, calls=%fused_computation.10 | convolution fusion | flops 2348810240 | bytes 8585216 | tf_op jit(solution)/shard_map/tsecd,edf->tsecf/dot_general | solution.py:297
  113.7 3.0 %fusion.54 = bf16[4,4,40,896]{3,2,1,0:T(8,128)(2,1)S(1)} fusion(bf16[1,2048,896]{2,1,0:T(8,128)(2,1)S(1)} %copy-done.7, bf16[4,4,1,40,2048]{4,3,1,0,2:T(8,128)(2,1)S(1)} %pad_maximum_fusion, f32[4,4,40,896]{3,2,1,0:T(8,128)S(1)} %fusion.5), kind=kOutput, calls=%fused_computation.49 | convolution fusion | flops 2352250880 | bytes 9732096 | tf_op jit(solution)/shard_map/tsecd,edf->tsecf/dot_general | solution.py:300
  116.7 4.4 %fusion = bf16[4,4,1,40,2048]{4,3,1,0,2:T(8,128)(2,1)} fusion(bf16[4,4,1,40,2048]{4,3,1,0,2:T(8,128)(2,1)S(1)} %collective-permute-done.7, bf16[4,4,40,896]{3,2,1,0:T(8,128)(2,1)S(1)} %fusion.54, bf16[1,896,2048]{2,1,0:T(8,128)(2,1)S(1)} %copy-done.8), kind=kOutput, calls=%fused_computation.5 | convolution fusion | flops 2355363840 | bytes 10059776 | tf_op jit(solution)/shard_map/tsecf,efd->tsecd/dot_general | solution.py:304
  122.3 51.5 %reduce-scatter.2.cloned.1.call-done = bf16[1,4,1,40,2048]{4,3,1,0,2:T(8,128)(2,1)} async-done(((bf16[4,4,1,40,2048]{4,3,1,0,2:T(8,128)(2,1)}), bf16[1,4,1,40,2048]{4,3,1,0,2:T(8,128)(2,1)}) %reduce-scatter.2.cloned.1.call-update) | async-done | bytes 655376 | tf_op jit(solution)/shard_map/reduce_scatter | solution.py:315
  174.9 1.5 collective-permute-start.8
  176.4 1.5 collective-permute-start.9
  179.5 4.4 %convolution_convert_fusion = bf16[2048,256]{1,0:T(8,128)(2,1)} fusion(bf16[2048,1024]{1,0:T(8,128)(2,1)} %all-gather.3.cloned.1.call-done, bf16[1024,256]{1,0:T(8,128)(2,1)S(1)} %copy-done), kind=kOutput, calls=%fused_computation.27 | convolution fusion | flops 1074266112 | bytes 5767168 | tf_op jit(solution)/shard_map/dot_general | solution.py:323
  183.9 1.4 collective-permute-done.9
  (80 shorter events, 14.6 us)
Async XLA Ops:
  7.2 172.3 %copy-start = (bf16[1024,256]{1,0:T(8,128)(2,1)S(1)}, bf16[1024,256]{1,0:T(8,128)(2,1)}, u32[]{:S(2)}) copy-start(bf16[1024,256]{1,0:T(8,128)(2,1)} %param.22) | copy-start | bytes 1572868
  7.2 3.1 %copy-start.2 = (bf16[512,2048]{1,0:T(8,128)(2,1)S(1)}, bf16[512,2048]{1,0:T(8,128)(2,1)}, u32[]{:S(2)}) copy-start(bf16[512,2048]{1,0:T(8,128)(2,1)} %param.23) | copy-start | bytes 6291460
  7.2 3.3 %copy-start.5 = (s32[512,2]{0,1:T(2,128)S(1)}, s32[512,2]{0,1:T(2,128)}, u32[]{:S(2)}) copy-start(s32[512,2]{0,1:T(2,128)} %param.25) | copy-start | bytes 12292
  7.2 113.9 %all-gather.3.cloned.1.call-start = ((), (), s32[]{:S(2)}) async-start(), calls=%async_computation.1 | async-start | bytes 4718592 | tf_op jit(solution)/shard_map/all_gather | solution.py:294
  7.3 7.8 %copy-start.4 = (f32[2048]{0:T(1024)S(1)}, f32[2048]{0:T(1024)}, u32[]{:S(2)}) copy-start(f32[2048]{0:T(1024)} %param.24) | copy-start | bytes 24580
  21.0 2.0 %copy-start.3 = (f32[2048,2]{0,1:T(2,128)S(1)}, f32[2048,2]{0,1:T(2,128)}, u32[]{:S(2)}) copy-start(f32[2048,2]{0,1:T(2,128)} %param.20) | copy-start | bytes 49156
  56.2 117.6 %reduce-scatter.2.cloned.1.call-start = ((), (), s32[]{:S(2)}) async-start(), calls=%async_computation.2 | async-start | bytes 3276800 | tf_op jit(solution)/shard_map/reduce_scatter | solution.py:315
  56.7 17.7 %collective-permute-start = (bf16[4,1,40,2048]{3,2,0,1:T(8,128)(2,1)S(1)}, bf16[4,1,40,2048]{3,2,0,1:T(8,128)(2,1)S(1)}, u32[]{:S(2)}, u32[]{:S(2)}) collective-permute-start(bf16[4,1,40,2048]{3,2,0,1:T(8,128)(2,1)S(1)} %get-tuple-element.25), channel_id=1, source_target_pairs={{0,8},{8,0},{16,24},{24,16},{1,9},{9,1},{17,25},{25,17},{2,10},{10... | collective-permute-start | bytes 1966088 | tf_op jit(solution)/shard_map/ppermute | solution.py:275
  57.4 28.5 %collective-permute-start.1 = (bf16[4,1,40,2048]{3,2,0,1:T(8,128)(2,1)S(1)}, bf16[4,1,40,2048]{3,2,0,1:T(8,128)(2,1)S(1)}, u32[]{:S(2)}, u32[]{:S(2)}) collective-permute-start(bf16[4,1,40,2048]{3,2,0,1:T(8,128)(2,1)S(1)} %get-tuple-element.24), channel_id=1, source_target_pairs={{0,16},{8,24},{16,0},{24,8},{1,17},{9,25},{17,1},{25,9},{2,18},{10... | collective-permute-start | bytes 1966088 | tf_op jit(solution)/shard_map/ppermute | solution.py:275
  58.8 27.1 %collective-permute-start.2 = (bf16[4,1,40,2048]{3,2,0,1:T(8,128)(2,1)S(1)}, bf16[4,1,40,2048]{3,2,0,1:T(8,128)(2,1)S(1)}, u32[]{:S(2)}, u32[]{:S(2)}) collective-permute-start(bf16[4,1,40,2048]{3,2,0,1:T(8,128)(2,1)S(1)} %get-tuple-element.23), channel_id=1, source_target_pairs={{0,24},{8,16},{16,8},{24,0},{1,25},{9,17},{17,9},{25,1},{2,26},{10... | collective-permute-start | bytes 1966088 | tf_op jit(solution)/shard_map/ppermute | solution.py:275
  60.3 26.5 %collective-permute-start.3 = (bf16[4,1,40,2048]{3,2,0,1:T(8,128)(2,1)S(1)}, bf16[4,1,40,2048]{3,2,0,1:T(8,128)(2,1)S(1)}, u32[]{:S(2)}, u32[]{:S(2)}) collective-permute-start(bf16[4,1,40,2048]{3,2,0,1:T(8,128)(2,1)S(1)} %get-tuple-element.22), channel_id=1, source_target_pairs={{0,1},{1,0},{2,3},{3,2},{4,5},{5,4},{6,7},{7,6},{8,9},{9,8},{10,11... | collective-permute-start | bytes 1966088 | tf_op jit(solution)/shard_map/ppermute | solution.py:279
  74.4 12.4 %collective-permute-start.4 = (bf16[4,1,40,2048]{3,2,0,1:T(8,128)(2,1)S(1)}, bf16[4,1,40,2048]{3,2,0,1:T(8,128)(2,1)S(1)}, u32[]{:S(2)}, u32[]{:S(2)}) collective-permute-start(bf16[4,1,40,2048]{3,2,0,1:T(8,128)(2,1)S(1)} %collective-permute-done), channel_id=1, source_target_pairs={{0,1},{1,0},{2,3},{3,2},{4,5},{5,4},{6,7},{7,6},{8,9},{9,8},{10,11... | collective-permute-start | bytes 1966088 | tf_op jit(solution)/shard_map/ppermute | solution.py:279
  85.9 2.4 %collective-permute-start.5 = (bf16[4,1,40,2048]{3,2,0,1:T(8,128)(2,1)S(1)}, bf16[4,1,40,2048]{3,2,0,1:T(8,128)(2,1)S(1)}, u32[]{:S(2)}, u32[]{:S(2)}) collective-permute-start(bf16[4,1,40,2048]{3,2,0,1:T(8,128)(2,1)S(1)} %collective-permute-done.1), channel_id=1, source_target_pairs={{0,1},{1,0},{2,3},{3,2},{4,5},{5,4},{6,7},{7,6},{8,9},{9,8},{10,11... | collective-permute-start | bytes 1966088 | tf_op jit(solution)/shard_map/ppermute | solution.py:279
  85.9 3.4 %collective-permute-start.6 = (bf16[4,1,40,2048]{3,2,0,1:T(8,128)(2,1)S(1)}, bf16[4,1,40,2048]{3,2,0,1:T(8,128)(2,1)S(1)}, u32[]{:S(2)}, u32[]{:S(2)}) collective-permute-start(bf16[4,1,40,2048]{3,2,0,1:T(8,128)(2,1)S(1)} %collective-permute-done.2), channel_id=1, source_target_pairs={{0,1},{1,0},{2,3},{3,2},{4,5},{5,4},{6,7},{7,6},{8,9},{9,8},{10,11... | collective-permute-start | bytes 1966088 | tf_op jit(solution)/shard_map/ppermute | solution.py:279
  89.3 3.0 %copy-start.6 = (bf16[1,2048,896]{2,1,0:T(8,128)(2,1)S(1)}, bf16[1,2048,896]{2,1,0:T(8,128)(2,1)}, u32[]{:S(2)}) copy-start(bf16[1,2048,896]{2,1,0:T(8,128)(2,1)} %param.27) | copy-start | bytes 11010052
  89.7 1.5 copy-start.1
  108.4 5.3 %copy-start.7 = (bf16[1,2048,896]{2,1,0:T(8,128)(2,1)S(1)}, bf16[1,2048,896]{2,1,0:T(8,128)(2,1)}, u32[]{:S(2)}) copy-start(bf16[1,2048,896]{2,1,0:T(8,128)(2,1)} %param.28) | copy-start | bytes 11010052
  108.4 8.3 %collective-permute-start.7 = (bf16[4,4,1,40,2048]{4,3,1,0,2:T(8,128)(2,1)}, bf16[4,4,1,40,2048]{4,3,1,0,2:T(8,128)(2,1)S(1)}, u32[]{:S(2)}, u32[]{:S(2)}) collective-permute-start(bf16[4,4,1,40,2048]{4,3,1,0,2:T(8,128)(2,1)} %fusion.22), channel_id=1, source_target_pairs={{0,1},{1,0},{2,3},{3,2},{4,5},{5,4},{6,7},{7,6},{8,9},{9,8},{10,11... | collective-permute-start | bytes 7864328 | tf_op jit(solution)/shard_map/ppermute | solution.py:312
  113.7 3.0 %copy-start.8 = (bf16[1,896,2048]{2,1,0:T(8,128)(2,1)S(1)}, bf16[1,896,2048]{2,1,0:T(8,128)(2,1)}, u32[]{:S(2)}) copy-start(bf16[1,896,2048]{2,1,0:T(8,128)(2,1)} %param.29) | copy-start | bytes 11010052
  174.9 9.0 %collective-permute-start.8 = (bf16[1,40,2048]{2,1,0:T(8,128)(2,1)S(1)}, bf16[1,40,2048]{2,1,0:T(8,128)(2,1)S(1)}, u32[]{:S(2)}, u32[]{:S(2)}) collective-permute-start(bf16[1,40,2048]{2,1,0:T(8,128)(2,1)S(1)} %get-tuple-element.28), channel_id=1, source_target_pairs={{0,8},{8,0},{16,24},{24,16},{1,9},{9,1},{17,25},{25,17},{2,10},{10... | collective-permute-start | bytes 491528 | tf_op jit(solution)/shard_map/ppermute | solution.py:330
  176.4 8.8 %collective-permute-start.9 = (bf16[1,40,2048]{2,1,0:T(8,128)(2,1)S(1)}, bf16[1,40,2048]{2,1,0:T(8,128)(2,1)S(1)}, u32[]{:S(2)}, u32[]{:S(2)}) collective-permute-start(bf16[1,40,2048]{2,1,0:T(8,128)(2,1)S(1)} %get-tuple-element.27), channel_id=1, source_target_pairs={{0,16},{8,24},{16,0},{24,8},{1,17},{9,25},{17,1},{25,9},{2,18},{10... | collective-permute-start | bytes 491528 | tf_op jit(solution)/shard_map/ppermute | solution.py:330
  178.8 6.4 %collective-permute-start.10 = (bf16[1,40,2048]{2,1,0:T(8,128)(2,1)S(1)}, bf16[1,40,2048]{2,1,0:T(8,128)(2,1)S(1)}, u32[]{:S(2)}, u32[]{:S(2)}) collective-permute-start(bf16[1,40,2048]{2,1,0:T(8,128)(2,1)S(1)} %slice_bitcast_fusion), channel_id=1, source_target_pairs={{0,24},{8,16},{16,8},{24,0},{1,25},{9,17},{17,9},{25,1},{2,26},{10... | collective-permute-start | bytes 491528 | tf_op jit(solution)/shard_map/ppermute | solution.py:330
Sparse Core Ops, SparseCore 0:
  56.4 48.0 all-gather.2
  121.3 52.4 reduce-scatter.1
where the time goes:
time: 195 us
  waiting for transfers between devices  81.1 us (42%)
  matrix products  33 us (17%)
  Pallas kernels  20.3 us (10%)
  local copies, waits for them, and re-layouts  16.6 us (9%)
  between operations  14.4 us (7%)
  blocking collectives  11.6 us (6%)
  other arithmetic  9.47 us (5%)
  starting transfers between devices  8.09 us (4%)
    reduce_scatter x1, waiting for transfers between devices, on_device(): lax.psum_scatter(product, 'tp', scatter_dimension=0, tiled=True, axis_ind...  51.5 us
    ppermute x6, waiting for transfers between devices, on_device(): block = lax.ppermute(block, 'ep', [(i, i ^ step) for i in range(places)])  27.1 us
    dot_general x2, matrix products, experts(): jnp.einsum('tsecf,efd->tsecd', hidden, expert_down_weight, preferred_elem...  16.2 us
    pallas_call x1, Pallas kernels, local_recurrence(): pl.pallas_call(functools.partial(local_kernel, heads), grid=(length // CH...  15.7 us
    all_gather x1, blocking collectives, on_device(): carries = lax.all_gather(carry, 'ep')  11.6 us
    dot_general x2, matrix products, experts(): jnp.einsum('tsecd,edf->tsecf', rows, expert_gate_weight, preferred_elemen...  9.36 us
    ppermute x6, starting transfers between devices, on_device(): block = lax.ppermute(block, 'ep', [(i, i ^ step) for i in range(places)])  7.17 us
    pallas_call x1, Pallas kernels, gated_output(): pl.pallas_call(functools.partial(gate_kernel, heads, carries.shape[0]), g...  4.65 us
  transfers between devices with their start and end apart: 13, of which 6 were waited for; matrix products, arithmetic and copies ran while one was open for 18% of the time, Pallas kernels for 0%

commit v1 on v0

--- a/solution.py
+++ b/solution.py
@@ -229,7 +229,7 @@
     return filled.reshape(groups, experts_all, capacity, -1)
 
 
-def on_device(
+def general(
     query_preactivation,
     forget_preactivation,
     value_input_rows,
@@ -345,6 +345,636 @@
     return (mixer_output_first, combined.astype(jnp.bfloat16))
 
 
+MESH = pl.DeviceIdType.MESH
+LANES = 128
+ROW_CHUNKS = 4
+
+
+def fused_kernel(
+    idx_ref, weight_ref, norm_gain_ref, gap_ref, extra_ref, head_gain_ref,
+    tok_hbm, q_hbm, f_hbm, v_hbm, g_hbm, wo_hbm, wg_hbm, wu_hbm, wd_hbm,
+    out_ref, moe_ref,
+    tok, q, f, v, gate, wo, wgu, wd,
+    send_rows, rows, hidden, pair_out, pair_in, psum, from_end, from_mate, from_inner,
+    result_out, results, combined, moe_buf,
+    state, base, carries, rec, qdec, held_state, mixed_all, out_acc,
+    load_sem, disp_send, disp_recv, dfwd_send, dfwd_recv, pair_send, pair_recv,
+    end_send, end_recv, mate_send, mate_recv, inner_send, inner_recv,
+    ret_send, ret_recv, swap_send, swap_recv, carry_send, carry_recv,
+    own_send, own_recv, ag_send, ag_recv, agf_send, agf_recv,
+):
+    f32, bf16 = jnp.float32, jnp.bfloat16
+    ep = lax.axis_index("ep")
+    tp = lax.axis_index("tp")
+    z, c = tp // 2, tp % 2
+    oc = 1 - c
+    mate = z + 1 - 2 * (z % 2)
+    is_end = (z == 0) | (z == 3)
+    is_inner = (z == 1) | (z == 2)
+    places = rows.shape[0]
+    steps = places
+    pairs = mixed_all.shape[0]
+    two = idx_ref.shape[1] // pairs
+    sub = two // 2
+    width = tok.shape[1]
+    hw = width // 2
+    rows_all = rows.shape[1]
+    cp = rows_all // pairs
+    cap = cp // 2
+    length, keys = q.shape
+    vals = v.shape[1]
+    heads = keys // KEY_DIM
+    blocks_f = wgu.shape[0]
+    vc = vals
+    ep_peer = [{"ep": ep ^ s} for s in range(places)]
+    z_peer = [{"tp": (z ^ x) * 2 + c} for x in range(pairs)]
+    partner = {"tp": z * 2 + oc}
+    mate_dev = {"tp": mate * 2 + c}
+    across_dev = {"tp": (pairs - 1 - z) * 2 + c}
+
+    def half(i):
+        return pl.ds(pl.multiple_of(i * hw, LANES), hw)
+
+    def vcols(i):
+        return pl.ds(pl.multiple_of(i * vc, LANES), vc)
+
+    def zrows(d, n=1):
+        return pl.ds(pl.multiple_of(d * cp, 16), n * cp)
+
+    def remote(src, dst, ssem, rsem, dev):
+        return pltpu.make_async_remote_copy(
+            src_ref=src, dst_ref=dst, send_sem=ssem, recv_sem=rsem, device_id=dev, device_id_type=MESH
+        )
+
+    loads = {}
+
+    def load(name, src, dst):
+        copy = pltpu.make_async_copy(src, dst, load_sem.at[len(loads)])
+        copy.start()
+        loads[name] = copy
+
+    for g in range(pairs):
+        part = pl.ds(g * two, two)
+        load(("tok", g), tok_hbm.at[part], tok.at[part])
+    for j in range(blocks_f):
+        cols = pl.ds(j * LANES, LANES)
+        load(("wg", j), wg_hbm.at[0, :, cols], wgu.at[j, :, pl.ds(0, LANES)])
+        load(("wu", j), wu_hbm.at[0, :, cols], wgu.at[j, :, pl.ds(LANES, LANES)])
+    load("wd", wd_hbm.at[0], wd)
+    load("q", q_hbm, q)
+    load("f", f_hbm, f)
+    load("v", v_hbm, v)
+    load("gate", g_hbm, gate)
+    load("wo", wo_hbm, wo)
+
+    barrier = pltpu.get_barrier_semaphore()
+    greet = ep_peer[1:] + z_peer[1:] + [partner]
+    for dev in greet:
+        pl.semaphore_signal(barrier, inc=1, device_id=dev, device_id_type=MESH)
+
+    tri_a = lax.broadcasted_iota(jnp.int32, (two, two), 0)
+    tri_b = lax.broadcasted_iota(jnp.int32, (two, two), 1)
+    earlier = jnp.where((tri_a < tri_b) & (tri_a // sub == tri_b // sub), 1.0, 0.0).astype(bf16)
+    lane_side = lax.broadcasted_iota(jnp.int32, (8, two), 1) // sub
+    slot_row = lax.broadcasted_iota(jnp.int32, (cp, two), 0).astype(f32)
+    expert_row = ep ^ lax.broadcasted_iota(jnp.int32, (8, two), 0)
+
+    def targets(lanes):
+        first = jnp.broadcast_to(idx_ref[0:1, lanes], (8, two)) == expert_row
+        second = jnp.broadcast_to(idx_ref[1:2, lanes], (8, two)) == expert_row
+        match = first | second
+        before = jnp.dot(jnp.where(match, 1.0, 0.0).astype(bf16), earlier, preferred_element_type=f32)
+        where_to = jnp.where(match, before + (lane_side * cap).astype(f32), -1.0)
+        return where_to, first, second
+
+    for g in range(pairs):
+        part = slice(g * two, (g + 1) * two)
+        loads[("tok", g)].wait()
+        tokens = tok[part, :].astype(f32)
+        factor = lax.rsqrt(jnp.mean(tokens * tokens, axis=-1, keepdims=True) + epsilon)
+        tok[part, :] = (tokens * factor * norm_gain_ref[...]).astype(bf16)
+        where_to, _, _ = targets(slice(g * two, (g + 1) * two))
+        onehots = [
+            jnp.where(slot_row == where_to[s : s + 1, :], 1.0, 0.0).astype(bf16) for s in range(places)
+        ]
+        rows[0, g * cp : (g + 1) * cp, :] = jnp.dot(
+            onehots[0], tok[part, :], preferred_element_type=f32
+        ).astype(bf16)
+        own_half = tok[part, half(c)]
+        for s in range(1, places):
+            send_rows[s - 1, g * cp : (g + 1) * cp, :] = jnp.dot(
+                onehots[s], own_half, preferred_element_type=f32
+            ).astype(bf16)
+
+    pl.semaphore_wait(barrier, len(greet))
+
+    def dispatch(s):
+        return remote(
+            send_rows.at[s - 1], rows.at[s, :, half(c)], disp_send.at[s - 1], disp_recv.at[s - 1], ep_peer[s]
+        )
+
+    def dispatch_forward(s):
+        return remote(
+            rows.at[s, :, half(c)], rows.at[s, :, half(c)], dfwd_send.at[s - 1], dfwd_recv.at[s - 1], partner
+        )
+
+    def dispatch_forward_in(s):
+        return remote(
+            rows.at[s, :, half(oc)], rows.at[s, :, half(oc)], dfwd_send.at[s - 1], dfwd_recv.at[s - 1], partner
+        )
+
+    for s in range(1, places):
+        dispatch(s).start()
+
+    def forward(s):
+        dispatch(s).wait_recv()
+        dispatch_forward(s).start()
+
+    def pair_copy(s):
+        return remote(pair_out.at[s], pair_in.at[s], pair_send.at[s], pair_recv.at[s], partner)
+
+    def moe(s):
+        if s:
+            dispatch_forward_in(s).wait_recv()
+
+        def gate_up(j, _):
+            acc = jnp.dot(rows[s], wgu[j], preferred_element_type=f32)
+            part, up = acc[:, :LANES], acc[:, LANES:]
+            value = part / (1.0 + jnp.exp(-part)) * up
+            hidden[:, pl.ds(pl.multiple_of(j * LANES, LANES), LANES)] = value.astype(bf16)
+            return 0
+
+        lax.fori_loop(0, blocks_f, gate_up, 0)
+        tile = min(256, hw)
+
+        def down(dst, side):
+            def body(j, _):
+                start = pl.multiple_of(side * hw + j * tile, LANES)
+                acc = jnp.dot(hidden[...], wd[:, pl.ds(start, tile)], preferred_element_type=f32)
+                dst[s, :, pl.ds(pl.multiple_of(j * tile, LANES), tile)] = acc.astype(bf16)
+                return 0
+
+            lax.fori_loop(0, hw // tile, body, 0)
+
+        if s == 0:
+            loads["wd"].wait()
+        down(pair_out, oc)
+        pair_copy(s).start()
+        down(psum, c)
+
+    far = (1 - z // 2) * 2
+
+    def end_copy(s):
+        return remote(psum.at[s, zrows(far, 2)], from_end.at[s], end_send.at[s], end_recv.at[s], mate_dev)
+
+    def mate_copy(s):
+        return remote(psum.at[s, zrows(mate)], from_mate.at[s], mate_send.at[s], mate_recv.at[s], mate_dev)
+
+    def inner_copy(s):
+        return remote(psum.at[s, zrows(far, 2)], from_inner.at[s], inner_send.at[s], inner_recv.at[s], across_dev)
+
+    def add_into(s, at, other):
+        psum[s, at, :] = (psum[s, at, :].astype(f32) + other.astype(f32)).astype(bf16)
+
+    def stage1(s):
+        pair_copy(s).wait_recv()
+
+        def body(k, _):
+            at = zrows(k)
+            add_into(s, at, pair_in[s, at, :])
+            return 0
+
+        lax.fori_loop(0, pairs, body, 0)
+
+        @pl.when(is_end)
+        def _():
+            end_copy(s).start()
+            mate_copy(s).start()
+
+    def stage2(s):
+        @pl.when(is_inner)
+        def _():
+            end_copy(s).wait_recv()
+
+            def body(k, _):
+                add_into(s, zrows(far + k), from_end[s, zrows(k), :])
+                return 0
+
+            lax.fori_loop(0, 2, body, 0)
+            inner_copy(s).start()
+
+    def stage3(s):
+        @pl.when(is_inner)
+        def _():
+            inner_copy(s).wait_recv()
+            add_into(s, zrows(mate), from_inner[s, zrows(mate % 2), :])
+            mate_copy(s).start()
+
+    def result_copy(s):
+        return remote(
+            result_out.at[s], results.at[pl.ds(s * cp, cp)], ret_send.at[s - 1], ret_recv.at[s - 1], ep_peer[s]
+        )
+
+    def stage4(s):
+        mate_copy(s).wait_recv()
+        total = psum[s, zrows(z), :].astype(f32) + from_mate[s].astype(f32)
+        here = slice(s * cp, (s + 1) * cp)
+
+        def put(value):
+            if s:
+                result_out[s] = value.astype(bf16)
+            else:
+                results[here, :] = value.astype(bf16)
+
+        @pl.when(is_end)
+        def _():
+            put(total)
+
+        @pl.when(is_inner)
+        def _():
+            put(total + from_inner[s, zrows(z % 2), :].astype(f32))
+
+        if s:
+            result_copy(s).start()
+
+    def carry_copy(s):
+        return remote(carries.at[0], carries.at[s], carry_send.at[s - 1], carry_recv.at[s - 1], ep_peer[s])
+
+    def recurrence(services):
+        state[...] = jnp.zeros_like(state)
+        base[...] = jnp.zeros_like(base)
+        n = CHUNK
+        at = lax.broadcasted_iota(jnp.int32, (n, n), 0)
+        of = lax.broadcasted_iota(jnp.int32, (n, n), 1)
+        same = (at >= of) & (at // BLOCK_POSITIONS == of // BLOCK_POSITIONS)
+        lower = jnp.where(same, 1.0, 0.0).astype(bf16)
+        er = lax.broadcasted_iota(jnp.int32, (8, n), 0)
+        pick_row = lax.broadcasted_iota(jnp.int32, (8, keys), 0)
+        pick_head = lax.broadcasted_iota(jnp.int32, (8, keys), 1) // KEY_DIM
+        pick = jnp.where((pick_row % heads == pick_head) & (pick_row < 3 * heads), 1.0, 0.0).astype(bf16)
+        small = (BLOCK_POSITIONS, BLOCK_POSITIONS)
+        causal = lax.broadcasted_iota(jnp.int32, small, 0) >= lax.broadcasted_iota(jnp.int32, small, 1)
+        lane_head = lax.broadcasted_iota(jnp.int32, (BLOCK_POSITIONS, vals), 1) // VAL_DIM
+
+        def chunk(i, _):
+            for when, work in services.items():
+
+                @pl.when(i == when)
+                def _():
+                    work()
+
+            start = pl.multiple_of(i * n, n)
+            here = pl.ds(start, n)
+            qc = q[here, :].astype(f32)
+            qc = qc / (1.0 + jnp.exp(-qc))
+            key = gap_ref[...] / (1.0 + jnp.exp(f[here, :].astype(f32)))
+            terms = jnp.zeros((8, n), f32)
+            for h in range(heads):
+                value = jnp.broadcast_to(extra_ref[h : h + 1, here], (8, n))
+                one = value.astype(bf16).astype(f32)
+                second = (value - one).astype(bf16).astype(f32)
+                third = value - one - second
+                terms = jnp.where(er == h, one, terms)
+                terms = jnp.where(er == heads + h, second, terms)
+                terms = jnp.where(er == 2 * heads + h, third, terms)
+            extra = lax.dot_general(terms.astype(bf16), pick, TN, preferred_element_type=f32)
+            log_forget = jnp.log(1.0 - key) + extra
+            high = log_forget.astype(bf16)
+            low = (log_forget - high.astype(f32)).astype(bf16)
+            cumulative = jnp.dot(lower, high, preferred_element_type=f32) + jnp.dot(
+                lower, low, preferred_element_type=f32
+            )
+            held = [state[h] for h in range(heads)]
+            before = base[...]
+            mid_at = BLOCK_POSITIONS // 2
+            for b in range(n // BLOCK_POSITIONS):
+                part = slice(b * BLOCK_POSITIONS, (b + 1) * BLOCK_POSITIONS)
+                block = pl.ds(start + b * BLOCK_POSITIONS, BLOCK_POSITIONS)
+                cum = cumulative[part]
+                mid, last = cum[mid_at - 1 : mid_at], cum[BLOCK_POSITIONS - 1 :]
+                q_part = qc[part]
+                q_mid = (q_part * jnp.exp(cum - mid)).astype(bf16)
+                k_mid = (key[part] * jnp.exp(mid - cum)).astype(bf16)
+                qdec[block, :] = (q_part * jnp.exp(cum + before)).astype(bf16)
+                decay_mid, decay_last, decay_rest = jnp.exp(mid), jnp.exp(last), jnp.exp(last - mid)
+                before = before + last
+                values = v[block, :]
+                out = jnp.zeros((BLOCK_POSITIONS, vals), f32)
+                for h in range(heads):
+                    lanes = slice(h * KEY_DIM, (h + 1) * KEY_DIM)
+                    across = lax.dot_general(
+                        q_mid[:, lanes],
+                        (held[h] * decay_mid[:, lanes]).astype(bf16),
+                        NT,
+                        preferred_element_type=f32,
+                    )
+                    scores = lax.dot_general(q_mid[:, lanes], k_mid[:, lanes], NT, preferred_element_type=f32)
+                    scores = jnp.where(causal, scores, 0.0).astype(bf16)
+                    within = jnp.dot(scores, values, preferred_element_type=f32)
+                    out = jnp.where(lane_head == h, within + across, out)
+                    update = lax.dot_general(values, k_mid[:, lanes], TN, preferred_element_type=f32)
+                    held[h] = held[h] * decay_last[:, lanes] + update * decay_rest[:, lanes]
+                rec[block, :] = out
+            for h in range(heads):
+                state[h] = held[h]
+            base[...] = before
+            return 0
+
+        lax.fori_loop(0, length // n, chunk, 0)
+        own = [state[h, h * VAL_DIM : (h + 1) * VAL_DIM, :] for h in range(heads)]
+        carries[0, :VAL_DIM, :] = jnp.concatenate(own, axis=1).astype(bf16)
+        total = jnp.exp(base[...])
+        carries[0, VAL_DIM:, :] = jnp.broadcast_to(total, (16, keys)).astype(bf16)
+        for s in range(1, places):
+            carry_copy(s).start()
+
+    chunk_rows = length // ROW_CHUNKS
+
+    def rows_of(r):
+        return pl.ds(r * chunk_rows, chunk_rows)
+
+    def own_copy(r):
+        here = mixed_all.at[z, rows_of(r), vcols(c)]
+        return remote(here, here, own_send.at[r], own_recv.at[r], partner)
+
+    def own_in(r):
+        here = mixed_all.at[z, rows_of(r), vcols(oc)]
+        return remote(here, here, own_send.at[r], own_recv.at[r], partner)
+
+    def ag_copy(x, r):
+        here = mixed_all.at[z, rows_of(r), vcols(c)]
+        return remote(here, here, ag_send.at[x - 1, r], ag_recv.at[x - 1, r], z_peer[x])
+
+    def ag_in(x, r):
+        here = mixed_all.at[z ^ x, rows_of(r), vcols(c)]
+        return remote(here, here, ag_send.at[x - 1, r], ag_recv.at[x - 1, r], z_peer[x])
+
+    def ag_forward(x, r):
+        here = mixed_all.at[z ^ x, rows_of(r), vcols(c)]
+        return remote(here, here, agf_send.at[x - 1, r], agf_recv.at[x - 1, r], partner)
+
+    def ag_forward_in(x, r):
+        here = mixed_all.at[z ^ x, rows_of(r), vcols(oc)]
+        return remote(here, here, agf_send.at[x - 1, r], agf_recv.at[x - 1, r], partner)
+
+    def gated():
+        for s in range(1, places):
+            carry_copy(s).wait_recv()
+        total = jnp.zeros((VAL_DIM, keys), f32)
+        for i in range(places):
+            decay = carries[ep ^ i, VAL_DIM:, :].astype(f32)[:1]
+            joined = total * decay + carries[ep ^ i, :VAL_DIM, :].astype(f32)
+            total = jnp.where(i < ep, joined, total)
+        lane_head = lax.broadcasted_iota(jnp.int32, total.shape, 1) // KEY_DIM
+        for h in range(heads):
+            held_state[h * VAL_DIM : (h + 1) * VAL_DIM, :] = jnp.where(lane_head == h, total, 0.0).astype(bf16)
+        at = lax.broadcasted_iota(jnp.int32, (vals, vals), 0) // VAL_DIM
+        of = lax.broadcasted_iota(jnp.int32, (vals, vals), 1) // VAL_DIM
+        average = jnp.where(at == of, 1.0 / VAL_DIM, 0.0).astype(bf16)
+        for r in range(ROW_CHUNKS):
+            here = rows_of(r)
+            whole = rec[here, :] + lax.dot_general(
+                qdec[here, :], held_state[...], NT, preferred_element_type=f32
+            )
+            square = whole * whole
+            high = square.astype(bf16)
+            low = (square - high.astype(f32)).astype(bf16)
+            mean = jnp.dot(high, average, preferred_element_type=f32) + jnp.dot(
+                low, average, preferred_element_type=f32
+            )
+            opened = gate[here, :].astype(f32)
+            opened = opened / (1.0 + jnp.exp(-opened))
+            mixed = (whole * lax.rsqrt(mean + epsilon) * head_gain_ref[...] * opened).astype(bf16)
+            mixed_all[z, here, vcols(c)] = mixed
+            for x in range(1, pairs):
+                ag_copy(x, r).start()
+            own_copy(r).start()
+
+    def project(x, last):
+        kw = 2 * vc
+        weight = wo[pl.ds(pl.multiple_of((z ^ x) * kw, LANES), kw), :]
+        for r in range(ROW_CHUNKS):
+            if x:
+                ag_forward_in(x, r).wait_recv()
+            else:
+                own_in(r).wait_recv()
+            here = rows_of(r)
+            part = jnp.dot(mixed_all[z ^ x, here, :], weight, preferred_element_type=f32)
+            if x:
+                part = part + out_acc[here, :]
+            if last:
+                out_ref[here, :] = part.astype(bf16)
+            else:
+                out_acc[here, :] = part
+
+    def ag_pass(x):
+        for r in range(ROW_CHUNKS):
+            ag_in(x, r).wait_recv()
+            ag_forward(x, r).start()
+
+    def swap_copy():
+        return remote(
+            combined.at[pl.ds(pl.multiple_of(oc * sub, 16), sub)],
+            moe_buf.at[:, half(c)], swap_send.at[0], swap_recv.at[0], partner,
+        )
+
+    def swap_in():
+        return remote(
+            combined.at[pl.ds(pl.multiple_of(oc * sub, 16), sub)],
+            moe_buf.at[:, half(oc)], swap_send.at[0], swap_recv.at[0], partner,
+        )
+
+    def combine():
+        lanes = pl.ds(pl.multiple_of(z * two, LANES), two)
+        where_to, first, second = targets(lanes)
+        weight = jnp.where(first, jnp.broadcast_to(weight_ref[0:1, lanes], (8, two)), 0.0) + jnp.where(
+            second, jnp.broadcast_to(weight_ref[1:2, lanes], (8, two)), 0.0
+        )
+        high = weight.astype(bf16).astype(f32)
+        low = weight - high
+        picks = [slot_row == where_to[s : s + 1, :] for s in range(places)]
+        coarse = jnp.concatenate(
+            [jnp.where(picks[s], high[s : s + 1, :], 0.0).astype(bf16) for s in range(places)], axis=0
+        )
+        fine = jnp.concatenate(
+            [jnp.where(picks[s], low[s : s + 1, :], 0.0).astype(bf16) for s in range(places)], axis=0
+        )
+        for s in range(1, places):
+            result_copy(s).wait_recv()
+        total = lax.dot_general(coarse, results[...], TN, preferred_element_type=f32) + lax.dot_general(
+            fine, results[...], TN, preferred_element_type=f32
+        )
+        combined[...] = total.astype(bf16)
+        swap_copy().start()
+
+    def finish():
+        moe_buf[:, half(c)] = combined[pl.ds(pl.multiple_of(c * sub, 16), sub), :]
+        swap_in().wait_recv()
+        moe_ref[...] = moe_buf[...]
+
+    for j in range(blocks_f):
+        loads[("wg", j)].wait()
+        loads[("wu", j)].wait()
+    moe(0)
+    for name in ("q", "f", "v"):
+        loads[name].wait()
+    recurrence(
+        {
+            1: lambda: stage1(0),
+            3: lambda: stage2(0),
+            5: lambda: (stage3(0), forward(1)),
+            6: lambda: forward(2),
+        }
+    )
+    moe(1)
+    stage1(1)
+    loads["gate"].wait()
+    gated()
+    forward(3)
+    moe(2)
+    stage2(1)
+    stage1(2)
+    moe(3)
+    stage3(1)
+    stage2(2)
+    stage1(3)
+    loads["wo"].wait()
+    project(0, False)
+    stage4(0)
+    stage4(1)
+    stage3(2)
+    stage2(3)
+    ag_pass(1)
+    stage4(2)
+    project(1, False)
+    stage3(3)
+    ag_pass(2)
+    stage4(3)
+    project(2, False)
+    ag_pass(3)
+    combine()
+    project(3, True)
+    finish()
+
+    for s in range(1, places):
+        dispatch(s).wait_send()
+        dispatch_forward(s).wait_send()
+        carry_copy(s).wait_send()
+        result_copy(s).wait_send()
+    for s in range(places):
+        pair_copy(s).wait_send()
+        mate_copy(s).wait_send()
+
+        @pl.when(is_end)
+        def _():
+            end_copy(s).wait_send()
+
+        @pl.when(is_inner)
+        def _():
+            inner_copy(s).wait_send()
+
+    for r in range(ROW_CHUNKS):
+        own_copy(r).wait_send()
+        for x in range(1, pairs):
+            ag_copy(x, r).wait_send()
+            ag_forward(x, r).wait_send()
+    swap_copy().wait_send()
+
+
+def on_device(*arrays):
+    (
+        query, forget, values, gate, gap, extra, head_gain, out_weight,
+        tokens, norm_gain, index, weight, gate_weight, up_weight, down_weight,
+    ) = arrays
+    places, groups = lax.axis_size("ep"), lax.axis_size("tp")
+    pairs = groups // 2
+    length, keys = query.shape
+    vals = values.shape[1]
+    count, width = tokens.shape
+    hidden = gate_weight.shape[2]
+    sub = count // groups
+    experts_all = gate_weight.shape[0] * places
+    capacity = max(2, sub * TOPK * 5 // (4 * experts_all))
+    fits = (
+        places == 4
+        and groups == 8
+        and gate_weight.shape[0] == 1
+        and 2 * sub == LANES
+        and capacity % 8 == 0
+        and capacity <= sub
+        and vals == LANES
+        and keys == 2 * KEY_DIM
+        and length % (ROW_CHUNKS * CHUNK) == 0
+        and hidden % LANES == 0
+        and width % 512 == 0
+    )
+    if not fits:
+        return general(*arrays)
+    heads = keys // KEY_DIM
+    cp = 2 * capacity
+    rows_all = pairs * cp
+    hw = width // 2
+    features = out_weight.shape[1]
+    bf16, f32 = jnp.bfloat16, jnp.float32
+    vmem = pl.BlockSpec(memory_space=pltpu.VMEM)
+    anywhere = pl.BlockSpec(memory_space=pl.ANY)
+    dma = pltpu.SemaphoreType.DMA
+    scratch = [
+        pltpu.VMEM((count, width), bf16),
+        pltpu.VMEM((length, keys), bf16),
+        pltpu.VMEM((length, keys), bf16),
+        pltpu.VMEM((length, vals), bf16),
+        pltpu.VMEM((length, vals), bf16),
+        pltpu.VMEM(out_weight.shape, bf16),
+        pltpu.VMEM((hidden // LANES, width, 2 * LANES), bf16),
+        pltpu.VMEM((hidden, width), bf16),
+        pltpu.VMEM((places - 1, rows_all, hw), bf16),
+        pltpu.VMEM((places, rows_all, width), bf16),
+        pltpu.VMEM((rows_all, hidden), bf16),
+        pltpu.VMEM((places, rows_all, hw), bf16),
+        pltpu.VMEM((places, rows_all, hw), bf16),
+        pltpu.VMEM((places, rows_all, hw), bf16),
+        pltpu.VMEM((places, 2 * cp, hw), bf16),
+        pltpu.VMEM((places, cp, hw), bf16),
+        pltpu.VMEM((places, 2 * cp, hw), bf16),
+        pltpu.VMEM((places, cp, hw), bf16),
+        pltpu.VMEM((places * cp, hw), bf16),
+        pltpu.VMEM((2 * sub, hw), bf16),
+        pltpu.VMEM((sub, width), bf16),
+        pltpu.VMEM((heads, vals, KEY_DIM), f32),
+        pltpu.VMEM((1, keys), f32),
+        pltpu.VMEM((places, VAL_DIM + 16, keys), bf16),
+        pltpu.VMEM((length, vals), f32),
+        pltpu.VMEM((length, keys), bf16),
+        pltpu.VMEM((vals, keys), bf16),
+        pltpu.VMEM((pairs, length, 2 * vals), bf16),
+        pltpu.VMEM((length, features), f32),
+    ]
+    n_loads = pairs + 2 * (hidden // LANES) + 6
+    peers = places - 1
+    sems = [dma((n_loads,))]
+    sems += [dma((peers,))] * 4 + [dma((places,))] * 8 + [dma((peers,))] * 2 + [dma((1,))] * 2
+    sems += [dma((peers,))] * 2 + [dma((ROW_CHUNKS,))] * 2 + [dma((pairs - 1, ROW_CHUNKS))] * 4
+    return pl.pallas_call(
+        fused_kernel,
+        in_specs=[vmem] * 6 + [anywhere] * 9,
+        out_specs=[vmem, vmem],
+        out_shape=[
+            jax.ShapeDtypeStruct((length, features), bf16),
+            jax.ShapeDtypeStruct((sub, width), bf16),
+        ],
+        scratch_shapes=scratch + sems,
+        compiler_params=pltpu.CompilerParams(
+            collective_id=0, has_side_effects=True, vmem_limit_bytes=64 * 1024 * 1024 - 65536
+        ),
+        name="fused_layer",
+    )(
+        index.T, weight.T, norm_gain.reshape(1, width), gap.reshape(1, keys), extra.T,
+        head_gain.reshape(1, vals), tokens, query, forget, values, gate, out_weight,
+        gate_weight, up_weight, down_weight,
+    )
+
+
 def solution(mesh):
     placed = (
         P("ep", "tp"),

time: 195 us -> 135 us (0.69)
  Pallas kernels: 20.3 us -> 131 us
  waiting for transfers between devices: 81.1 us -> 0 us
  matrix products: 33 us -> 0 us
  between operations: 14.4 us -> 0.64 us
  local copies, waits for them, and re-layouts: 16.6 us -> 3.93 us
  blocking collectives: 11.6 us -> 0 us
  other arithmetic: 9.47 us -> 0 us
  starting transfers between devices: 8.09 us -> 0 us
    pallas_call x2 -> x1, Pallas kernels: 20.3 us -> 131 us  [on_device(): pl.pallas_call(fused_kernel, in_specs=[vmem] * 6 + [anywhere] * 9, out_sp...]
    reduce_scatter x1 -> x0, waiting for transfers between devices: 51.5 us -> none  [on_device(): lax.psum_scatter(product, 'tp', scatter_dimension=0, tiled=True, axis_ind...]
    dot_general x6 -> x0, matrix products: 33 us -> none  [the longest x2 16.2 us: experts(): jnp.einsum('tsecf,efd->tsecd', hidden, expert_down_weight, preferred_elem...]
    ppermute x11 -> x0, waiting for transfers between devices: 29.6 us -> none  [the longest x6 27.1 us: on_device(): block = lax.ppermute(block, 'ep', [(i, i ^ step) for i in range(places)])]
    all_gather x1 -> x0, blocking collectives: 11.6 us -> none  [on_device(): carries = lax.all_gather(carry, 'ep')]
    ppermute x11 -> x0, starting transfers between devices: 7.83 us -> none  [the longest x6 7.17 us: on_device(): block = lax.ppermute(block, 'ep', [(i, i ^ step) for i in range(places)])]
    convert_element_type x4 -> x0, other arithmetic: 5.82 us -> none  [the longest x1 2.97 us: norm_rows(): tokens_float = tokens.astype(jnp.float32)]
    gather x3 -> x0, local copies, waits for them, and re-layouts: 5.57 us -> none  [the longest x1 4.08 us: fill_slots(): gathered = rows_in.reshape(groups * sub_rows, -1)[jnp.maximum(lookup, 0)]]
  transfers between devices with their start and end apart: 13 -> 0, of which waited for: 6 -> 0; matrix products, arithmetic and copies ran while one was open for 18% -> 0% of each run, Pallas kernels for 0% -> 0%
where the time goes in v1:
time: 135 us
  Pallas kernels  131 us (97%)
  local copies, waits for them, and re-layouts  3.93 us (3%)
    pallas_call x1, Pallas kernels, on_device(): pl.pallas_call(fused_kernel, in_specs=[vmem] * 6 + [anywhere] * 9, out_sp...  131 us
    unnamed x2, local copies, waits for them, and re-layouts  3.93 us

profile of v1, /device:TPU:0, one launch (start us, length us, event | category | flops | bytes accessed | tf_op | source)
XLA Modules:
  0.0 135.2 jit_solution(15783415319080430244)
XLA Ops:
  0.6 130.7 %fused_layer.1 = (bf16[2048,256]{1,0:T(8,128)(2,1)}, bf16[64,2048]{1,0:T(8,128)(2,1)}) custom-call(s32[2,512]{1,0:T(2,128)} %bitcast.8, f32[2,512]{1,0:T(2,128)} %bitcast.9, f32[1,2048]{1,0:T(1,128)} %bitcast.7, f32[1,256]{1,0:T(1,128)} %bitcast.10, f32[2,2048]{1,0:T(2,128)} %bitcast.6, f32[1,128]{1,0:T(1,128)} %bitcast.11, bf16[512,2048]{1,0:T(8,128)(2,1)} %tok_hbm.1, ...), custom_call_target="tpu_custom_call" | custom-call | tf_op jit(solution)/shard_map/fused_layer/pallas_call | solution.py:958
  131.3 2.3 %copy.19 = bf16[2048,256]{1,0:T(8,128)(2,1)} copy(bf16[2048,256]{1,0:T(8,128)(2,1)} %get-tuple-element.4) | data formatting | bytes 2097152
  133.6 1.7 %copy.20 = bf16[64,2048]{1,0:T(8,128)(2,1)} copy(bf16[64,2048]{1,0:T(8,128)(2,1)} %get-tuple-element.5) | data formatting | bytes 524288

commit v2 on v1

--- a/solution.py
+++ b/solution.py
@@ -361,16 +361,17 @@
     load_sem, disp_send, disp_recv, dfwd_send, dfwd_recv, pair_send, pair_recv,
     end_send, end_recv, mate_send, mate_recv, inner_send, inner_recv,
     ret_send, ret_recv, swap_send, swap_recv, carry_send, carry_recv,
-    own_send, own_recv, ag_send, ag_recv, agf_send, agf_recv,
+    own_send, own_recv, right_send, left_send, ag_recv, agf_send, agf_recv,
 ):
     f32, bf16 = jnp.float32, jnp.bfloat16
     ep = lax.axis_index("ep")
     tp = lax.axis_index("tp")
     z, c = tp // 2, tp % 2
+    last_z = mixed_all.shape[0] - 1
     oc = 1 - c
     mate = z + 1 - 2 * (z % 2)
-    is_end = (z == 0) | (z == 3)
-    is_inner = (z == 1) | (z == 2)
+    is_end = (z == 0) | (z == last_z)
+    is_inner = (z > 0) & (z < last_z)
     places = rows.shape[0]
     steps = places
     pairs = mixed_all.shape[0]
@@ -447,6 +448,16 @@
         where_to = jnp.where(match, before + (lane_side * cap).astype(f32), -1.0)
         return where_to, first, second
 
+    def dispatch(s, g):
+        return remote(
+            send_rows.at[s - 1, zrows(g)], rows.at[s, zrows(g), half(c)],
+            disp_send.at[s - 1, g], disp_recv.at[s - 1, g], ep_peer[s],
+        )
+
+    def dispatch_forward(s, g, side):
+        here = rows.at[s, zrows(g), half(side)]
+        return remote(here, here, dfwd_send.at[s - 1, g], dfwd_recv.at[s - 1, g], partner)
+
     for g in range(pairs):
         part = slice(g * two, (g + 1) * two)
         loads[("tok", g)].wait()
@@ -457,45 +468,32 @@
         onehots = [
             jnp.where(slot_row == where_to[s : s + 1, :], 1.0, 0.0).astype(bf16) for s in range(places)
         ]
-        rows[0, g * cp : (g + 1) * cp, :] = jnp.dot(
-            onehots[0], tok[part, :], preferred_element_type=f32
-        ).astype(bf16)
         own_half = tok[part, half(c)]
         for s in range(1, places):
             send_rows[s - 1, g * cp : (g + 1) * cp, :] = jnp.dot(
                 onehots[s], own_half, preferred_element_type=f32
             ).astype(bf16)
-
-    pl.semaphore_wait(barrier, len(greet))
-
-    def dispatch(s):
-        return remote(
-            send_rows.at[s - 1], rows.at[s, :, half(c)], disp_send.at[s - 1], disp_recv.at[s - 1], ep_peer[s]
-        )
-
-    def dispatch_forward(s):
-        return remote(
-            rows.at[s, :, half(c)], rows.at[s, :, half(c)], dfwd_send.at[s - 1], dfwd_recv.at[s - 1], partner
-        )
-
-    def dispatch_forward_in(s):
-        return remote(
-            rows.at[s, :, half(oc)], rows.at[s, :, half(oc)], dfwd_send.at[s - 1], dfwd_recv.at[s - 1], partner
-        )
-
-    for s in range(1, places):
-        dispatch(s).start()
-
-    def forward(s):
-        dispatch(s).wait_recv()
-        dispatch_forward(s).start()
+        if g == 0:
+            pl.semaphore_wait(barrier, len(greet))
+        for s in (1, 2):
+            dispatch(s, g).start()
+        rows[0, g * cp : (g + 1) * cp, :] = jnp.dot(
+            onehots[0], tok[part, :], preferred_element_type=f32
+        ).astype(bf16)
+    for g in range(pairs):
+        dispatch(3, g).start()
+
+    def forward(s, g):
+        dispatch(s, g).wait_recv()
+        dispatch_forward(s, g, c).start()
 
     def pair_copy(s):
         return remote(pair_out.at[s], pair_in.at[s], pair_send.at[s], pair_recv.at[s], partner)
 
     def moe(s):
         if s:
-            dispatch_forward_in(s).wait_recv()
+            for g in range(pairs):
+                dispatch_forward(s, g, oc).wait_recv()
 
         def gate_up(j, _):
             acc = jnp.dot(rows[s], wgu[j], preferred_element_type=f32)
@@ -504,7 +502,7 @@
             hidden[:, pl.ds(pl.multiple_of(j * LANES, LANES), LANES)] = value.astype(bf16)
             return 0
 
-        lax.fori_loop(0, blocks_f, gate_up, 0)
+        lax.fori_loop(0, blocks_f, gate_up, 0, unroll=True)
         tile = min(256, hw)
 
         def down(dst, side):
@@ -514,7 +512,7 @@
                 dst[s, :, pl.ds(pl.multiple_of(j * tile, LANES), tile)] = acc.astype(bf16)
                 return 0
 
-            lax.fori_loop(0, hw // tile, body, 0)
+            lax.fori_loop(0, hw // tile, body, 0, unroll=True)
 
         if s == 0:
             loads["wd"].wait()
@@ -549,33 +547,36 @@
         @pl.when(is_end)
         def _():
             end_copy(s).start()
-            mate_copy(s).start()
 
     def stage2(s):
-        @pl.when(is_inner)
-        def _():
-            end_copy(s).wait_recv()
-
-            def body(k, _):
-                add_into(s, zrows(far + k), from_end[s, zrows(k), :])
-                return 0
-
-            lax.fori_loop(0, 2, body, 0)
-            inner_copy(s).start()
+        end_copy(s).wait_recv()
+
+        def body(k, _):
+            add_into(s, zrows(far + k), from_end[s, zrows(k), :])
+            return 0
+
+        lax.fori_loop(0, 2, body, 0)
+        inner_copy(s).start()
 
     def stage3(s):
-        @pl.when(is_inner)
-        def _():
-            inner_copy(s).wait_recv()
-            add_into(s, zrows(mate), from_inner[s, zrows(mate % 2), :])
-            mate_copy(s).start()
+        inner_copy(s).wait_recv()
+        add_into(s, zrows(mate), from_inner[s, zrows(mate % 2), :])
+        mate_copy(s).start()
+
+    def inner(work):
+        def run():
+            @pl.when(is_inner)
+            def _():
+                work()
+
+        return run
 
     def result_copy(s):
         return remote(
             result_out.at[s], results.at[pl.ds(s * cp, cp)], ret_send.at[s - 1], ret_recv.at[s - 1], ep_peer[s]
         )
 
-    def stage4(s):
+    def stage4(s, inside):
         mate_copy(s).wait_recv()
         total = psum[s, zrows(z), :].astype(f32) + from_mate[s].astype(f32)
         here = slice(s * cp, (s + 1) * cp)
@@ -586,13 +587,9 @@
             else:
                 results[here, :] = value.astype(bf16)
 
-        @pl.when(is_end)
-        def _():
-            put(total)
-
-        @pl.when(is_inner)
-        def _():
-            put(total + from_inner[s, zrows(z % 2), :].astype(f32))
+        if inside:
+            total = total + from_inner[s, zrows(z % 2), :].astype(f32)
+        put(total)
 
         if s:
             result_copy(s).start()
@@ -693,29 +690,51 @@
     def rows_of(r):
         return pl.ds(r * chunk_rows, chunk_rows)
 
-    def own_copy(r):
-        here = mixed_all.at[z, rows_of(r), vcols(c)]
+    def own_copy(r, side):
+        here = mixed_all.at[z, side, rows_of(r)]
         return remote(here, here, own_send.at[r], own_recv.at[r], partner)
 
-    def own_in(r):
-        here = mixed_all.at[z, rows_of(r), vcols(oc)]
-        return remote(here, here, own_send.at[r], own_recv.at[r], partner)
-
-    def ag_copy(x, r):
-        here = mixed_all.at[z, rows_of(r), vcols(c)]
-        return remote(here, here, ag_send.at[x - 1, r], ag_recv.at[x - 1, r], z_peer[x])
-
-    def ag_in(x, r):
-        here = mixed_all.at[z ^ x, rows_of(r), vcols(c)]
-        return remote(here, here, ag_send.at[x - 1, r], ag_recv.at[x - 1, r], z_peer[x])
-
-    def ag_forward(x, r):
-        here = mixed_all.at[z ^ x, rows_of(r), vcols(c)]
-        return remote(here, here, agf_send.at[x - 1, r], agf_recv.at[x - 1, r], partner)
-
-    def ag_forward_in(x, r):
-        here = mixed_all.at[z ^ x, rows_of(r), vcols(oc)]
-        return remote(here, here, agf_send.at[x - 1, r], agf_recv.at[x - 1, r], partner)
+    def hop_right(src, r):
+        here = mixed_all.at[src, c, rows_of(r)]
+        to = {"tp": jnp.minimum(z + 1, last_z) * 2 + c}
+        return remote(here, here, right_send.at[src, r], ag_recv.at[src, r], to)
+
+    def hop_left(src, r):
+        here = mixed_all.at[src, c, rows_of(r)]
+        to = {"tp": jnp.maximum(z - 1, 0) * 2 + c}
+        return remote(here, here, left_send.at[src, r], ag_recv.at[src, r], to)
+
+    def ag_forward(src, r, side):
+        here = mixed_all.at[src, side, rows_of(r)]
+        return remote(here, here, agf_send.at[src, r], agf_recv.at[src, r], partner)
+
+    def source(j, inside):
+        at = (None, 2, 0, 3)[j] if inside else j
+        return jnp.where(z < 2, at, last_z - at)
+
+    def start_own(r):
+        @pl.when(z < last_z)
+        def _():
+            hop_right(z, r).start()
+
+        @pl.when(z > 0)
+        def _():
+            hop_left(z, r).start()
+
+    def ag_step(j, inside, r):
+        src = source(j, inside)
+        hop_right(src, r).wait_recv()
+        if inside:
+
+            @pl.when(src < z)
+            def _():
+                hop_right(src, r).start()
+
+            @pl.when(src > z)
+            def _():
+                hop_left(src, r).start()
+
+        ag_forward(src, r, c).start()
 
     def gated():
         for s in range(1, places):
@@ -745,32 +764,30 @@
             opened = gate[here, :].astype(f32)
             opened = opened / (1.0 + jnp.exp(-opened))
             mixed = (whole * lax.rsqrt(mean + epsilon) * head_gain_ref[...] * opened).astype(bf16)
-            mixed_all[z, here, vcols(c)] = mixed
-            for x in range(1, pairs):
-                ag_copy(x, r).start()
-            own_copy(r).start()
-
-    def project(x, last):
-        kw = 2 * vc
-        weight = wo[pl.ds(pl.multiple_of((z ^ x) * kw, LANES), kw), :]
-        for r in range(ROW_CHUNKS):
-            if x:
-                ag_forward_in(x, r).wait_recv()
-            else:
-                own_in(r).wait_recv()
-            here = rows_of(r)
-            part = jnp.dot(mixed_all[z ^ x, here, :], weight, preferred_element_type=f32)
-            if x:
-                part = part + out_acc[here, :]
-            if last:
-                out_ref[here, :] = part.astype(bf16)
-            else:
-                out_acc[here, :] = part
-
-    def ag_pass(x):
-        for r in range(ROW_CHUNKS):
-            ag_in(x, r).wait_recv()
-            ag_forward(x, r).start()
+            mixed_all[z, c, here, :] = mixed
+
+            @pl.when(is_inner)
+            def _():
+                start_own(r)
+
+            own_copy(r, c).start()
+
+    def project(j, inside, r):
+        src = source(j, inside) if j else z
+        if j:
+            ag_forward(src, r, oc).wait_recv()
+        else:
+            own_copy(r, oc).wait_recv()
+        here = rows_of(r)
+        weight = wo[pl.ds(pl.multiple_of(src * 2 * vc, LANES), 2 * vc), :]
+        both = jnp.concatenate([mixed_all[src, 0, here, :], mixed_all[src, 1, here, :]], axis=1)
+        part = jnp.dot(both, weight, preferred_element_type=f32)
+        if j:
+            part = part + out_acc[here, :]
+        if j == last_z:
+            out_ref[here, :] = part.astype(bf16)
+        else:
+            out_acc[here, :] = part
 
     def swap_copy():
         return remote(
@@ -812,53 +829,93 @@
         swap_in().wait_recv()
         moe_ref[...] = moe_buf[...]
 
+    chunks = range(ROW_CHUNKS)
     for j in range(blocks_f):
         loads[("wg", j)].wait()
         loads[("wu", j)].wait()
     moe(0)
     for name in ("q", "f", "v"):
         loads[name].wait()
-    recurrence(
-        {
-            1: lambda: stage1(0),
-            3: lambda: stage2(0),
-            5: lambda: (stage3(0), forward(1)),
-            6: lambda: forward(2),
-        }
-    )
+
+    def take(s):
+        for g in range(pairs):
+            forward(s, g)
+
+    recurrence({1: lambda: stage1(0), 6: inner(lambda: stage2(0))})
+    take(1)
+    take(2)
     moe(1)
-    stage1(1)
     loads["gate"].wait()
     gated()
-    forward(3)
+    stage1(1)
+    inner(lambda: stage3(0))()
     moe(2)
-    stage2(1)
+    take(3)
     stage1(2)
     moe(3)
-    stage3(1)
-    stage2(2)
+    loads["wo"].wait()
     stage1(3)
-    loads["wo"].wait()
-    project(0, False)
-    stage4(0)
-    stage4(1)
-    stage3(2)
-    stage2(3)
-    ag_pass(1)
-    stage4(2)
-    project(1, False)
-    stage3(3)
-    ag_pass(2)
-    stage4(3)
-    project(2, False)
-    ag_pass(3)
+
+    @pl.when(is_end)
+    def _():
+        for r in chunks:
+            start_own(r)
+        for s in range(places):
+            mate_copy(s).start()
+        for r in chunks:
+            project(0, False, r)
+            ag_step(1, False, r)
+        stage4(0, False)
+        for r in chunks:
+            ag_step(2, False, r)
+            project(1, False, r)
+        stage4(1, False)
+        stage4(2, False)
+        for r in chunks:
+            project(2, False, r)
+        for r in (0, 1):
+            ag_step(3, False, r)
+        stage4(3, False)
+        for r in (2, 3):
+            ag_step(3, False, r)
+        for r in chunks:
+            project(3, False, r)
+
+    @pl.when(is_inner)
+    def _():
+        stage2(1)
+        for r in chunks:
+            project(0, True, r)
+            ag_step(1, True, r)
+        stage2(2)
+        stage3(1)
+        for r in chunks:
+            project(1, True, r)
+        stage2(3)
+        ag_step(2, True, 0)
+        stage3(2)
+        ag_step(2, True, 1)
+        ag_step(3, True, 0)
+        ag_step(2, True, 2)
+        ag_step(3, True, 1)
+        stage3(3)
+        ag_step(2, True, 3)
+        ag_step(3, True, 2)
+        for r in chunks:
+            project(2, True, r)
+        ag_step(3, True, 3)
+        for s in range(places):
+            stage4(s, True)
+        for r in chunks:
+            project(3, True, r)
+
     combine()
-    project(3, True)
     finish()
 
     for s in range(1, places):
-        dispatch(s).wait_send()
-        dispatch_forward(s).wait_send()
+        for g in range(pairs):
+            dispatch(s, g).wait_send()
+            dispatch_forward(s, g, c).wait_send()
         carry_copy(s).wait_send()
         result_copy(s).wait_send()
     for s in range(places):
@@ -873,11 +930,22 @@
         def _():
             inner_copy(s).wait_send()
 
-    for r in range(ROW_CHUNKS):
-        own_copy(r).wait_send()
-        for x in range(1, pairs):
-            ag_copy(x, r).wait_send()
-            ag_forward(x, r).wait_send()
+    for r in chunks:
+        own_copy(r, c).wait_send()
+        for src in range(pairs):
+
+            @pl.when((src <= z) & (z < last_z))
+            def _():
+                hop_right(src, r).wait_send()
+
+            @pl.when((src >= z) & (z > 0))
+            def _():
+                hop_left(src, r).wait_send()
+
+            @pl.when(src != z)
+            def _():
+                ag_forward(src, r, c).wait_send()
+
     swap_copy().wait_send()
 
 
@@ -947,14 +1015,14 @@
         pltpu.VMEM((length, vals), f32),
         pltpu.VMEM((length, keys), bf16),
         pltpu.VMEM((vals, keys), bf16),
-        pltpu.VMEM((pairs, length, 2 * vals), bf16),
+        pltpu.VMEM((pairs, 2, length, vals), bf16),
         pltpu.VMEM((length, features), f32),
     ]
     n_loads = pairs + 2 * (hidden // LANES) + 6
     peers = places - 1
     sems = [dma((n_loads,))]
-    sems += [dma((peers,))] * 4 + [dma((places,))] * 8 + [dma((peers,))] * 2 + [dma((1,))] * 2
-    sems += [dma((peers,))] * 2 + [dma((ROW_CHUNKS,))] * 2 + [dma((pairs - 1, ROW_CHUNKS))] * 4
+    sems += [dma((peers, pairs))] * 4 + [dma((places,))] * 8 + [dma((peers,))] * 2 + [dma((1,))] * 2
+    sems += [dma((peers,))] * 2 + [dma((ROW_CHUNKS,))] * 2 + [dma((pairs, ROW_CHUNKS))] * 5
     return pl.pallas_call(
         fused_kernel,
         in_specs=[vmem] * 6 + [anywhere] * 9,

time: 135 us -> 106 us (0.79)
  Pallas kernels: 131 us -> 101 us
    pallas_call x1, Pallas kernels: 131 us -> 101 us  [on_device(): pl.pallas_call(fused_kernel, in_specs=[vmem] * 6 + [anywhere] * 9, out_sp...]
where the time goes in v2:
time: 106 us
  Pallas kernels  101 us (95%)
  local copies, waits for them, and re-layouts  3.93 us (4%)
    pallas_call x1, Pallas kernels, on_device(): pl.pallas_call(fused_kernel, in_specs=[vmem] * 6 + [anywhere] * 9, out_sp...  101 us
    unnamed x2, local copies, waits for them, and re-layouts  3.93 us

profile of v2, /device:TPU:0, one launch (start us, length us, event | category | flops | bytes accessed | tf_op | source)
XLA Modules:
  0.0 105.7 jit_solution(588836975548899996)
XLA Ops:
  0.6 101.1 %fused_layer.1 = (bf16[2048,256]{1,0:T(8,128)(2,1)}, bf16[64,2048]{1,0:T(8,128)(2,1)}) custom-call(s32[2,512]{1,0:T(2,128)} %bitcast.8, f32[2,512]{1,0:T(2,128)} %bitcast.9, f32[1,2048]{1,0:T(1,128)} %bitcast.7, f32[1,256]{1,0:T(1,128)} %bitcast.10, f32[2,2048]{1,0:T(2,128)} %bitcast.6, f32[1,128]{1,0:T(1,128)} %bitcast.11, bf16[512,2048]{1,0:T(8,128)(2,1)} %tok_hbm.1, ...), custom_call_target="tpu_custom_call" | custom-call | tf_op jit(solution)/shard_map/fused_layer/pallas_call | solution.py:1026
  101.8 2.3 %copy.19 = bf16[2048,256]{1,0:T(8,128)(2,1)} copy(bf16[2048,256]{1,0:T(8,128)(2,1)} %get-tuple-element.4) | data formatting | bytes 2097152
  104.1 1.7 %copy.20 = bf16[64,2048]{1,0:T(8,128)(2,1)} copy(bf16[64,2048]{1,0:T(8,128)(2,1)} %get-tuple-element.5) | data formatting | bytes 524288

commit v3 on v2

--- a/solution.py
+++ b/solution.py
@@ -351,17 +351,18 @@
 
 
 def fused_kernel(
-    idx_ref, weight_ref, norm_gain_ref, gap_ref, extra_ref, head_gain_ref,
+    idx_hbm, weight_hbm, norm_gain_hbm, gap_hbm, extra_hbm, head_gain_hbm,
     tok_hbm, q_hbm, f_hbm, v_hbm, g_hbm, wo_hbm, wg_hbm, wu_hbm, wd_hbm,
     out_ref, moe_ref,
+    idx_ref, weight_ref, norm_gain_ref, gap_ref, extra_ref, head_gain_ref,
     tok, q, f, v, gate, wo, wgu, wd,
     send_rows, rows, hidden, pair_out, pair_in, psum, from_end, from_mate, from_inner,
     result_out, results, combined, moe_buf,
-    state, base, carries, rec, qdec, held_state, mixed_all, out_acc,
+    state, base, carries, rec, qdec, held_state, mixed_all, out_acc, out_buf,
     load_sem, disp_send, disp_recv, dfwd_send, dfwd_recv, pair_send, pair_recv,
     end_send, end_recv, mate_send, mate_recv, inner_send, inner_recv,
     ret_send, ret_recv, swap_send, swap_recv, carry_send, carry_recv,
-    own_send, own_recv, right_send, left_send, ag_recv, agf_send, agf_recv,
+    own_send, own_recv, right_send, left_send, ag_recv, agf_send, agf_recv, out_sem,
 ):
     f32, bf16 = jnp.float32, jnp.bfloat16
     ep = lax.axis_index("ep")
@@ -388,11 +389,16 @@
     blocks_f = wgu.shape[0]
     vc = vals
     ep_peer = [{"ep": ep ^ s} for s in range(places)]
-    z_peer = [{"tp": (z ^ x) * 2 + c} for x in range(pairs)]
     partner = {"tp": z * 2 + oc}
     mate_dev = {"tp": mate * 2 + c}
     across_dev = {"tp": (pairs - 1 - z) * 2 + c}
 
+    pieces = 2
+    pw = hw // pieces
+
+    def piece(h):
+        return pl.ds(h * pw, pw)
+
     def half(i):
         return pl.ds(pl.multiple_of(i * hw, LANES), hw)
 
@@ -406,6 +412,18 @@
         return pltpu.make_async_remote_copy(
             src_ref=src, dst_ref=dst, send_sem=ssem, recv_sem=rsem, device_id=dev, device_id_type=MESH
         )
+
+    barrier = pltpu.get_barrier_semaphore()
+    for dev in ep_peer[1:] + [partner]:
+        pl.semaphore_signal(barrier, inc=1, device_id=dev, device_id_type=MESH)
+
+    @pl.when(z > 0)
+    def _():
+        pl.semaphore_signal(barrier, inc=1, device_id={"tp": tp - 2}, device_id_type=MESH)
+
+    @pl.when(z < last_z)
+    def _():
+        pl.semaphore_signal(barrier, inc=1, device_id={"tp": tp + 2}, device_id_type=MESH)
 
     loads = {}
 
@@ -414,6 +432,8 @@
         copy.start()
         loads[name] = copy
 
+    load("idx", idx_hbm, idx_ref)
+    load("norm_gain", norm_gain_hbm, norm_gain_ref)
     for g in range(pairs):
         part = pl.ds(g * two, two)
         load(("tok", g), tok_hbm.at[part], tok.at[part])
@@ -422,16 +442,15 @@
         load(("wg", j), wg_hbm.at[0, :, cols], wgu.at[j, :, pl.ds(0, LANES)])
         load(("wu", j), wu_hbm.at[0, :, cols], wgu.at[j, :, pl.ds(LANES, LANES)])
     load("wd", wd_hbm.at[0], wd)
+    load("weight", weight_hbm, weight_ref)
+    load("gap", gap_hbm, gap_ref)
+    load("extra", extra_hbm, extra_ref)
+    load("head_gain", head_gain_hbm, head_gain_ref)
     load("q", q_hbm, q)
     load("f", f_hbm, f)
     load("v", v_hbm, v)
     load("gate", g_hbm, gate)
     load("wo", wo_hbm, wo)
-
-    barrier = pltpu.get_barrier_semaphore()
-    greet = ep_peer[1:] + z_peer[1:] + [partner]
-    for dev in greet:
-        pl.semaphore_signal(barrier, inc=1, device_id=dev, device_id_type=MESH)
 
     tri_a = lax.broadcasted_iota(jnp.int32, (two, two), 0)
     tri_b = lax.broadcasted_iota(jnp.int32, (two, two), 1)
@@ -458,6 +477,8 @@
         here = rows.at[s, zrows(g), half(side)]
         return remote(here, here, dfwd_send.at[s - 1, g], dfwd_recv.at[s - 1, g], partner)
 
+    loads["idx"].wait()
+    loads["norm_gain"].wait()
     for g in range(pairs):
         part = slice(g * two, (g + 1) * two)
         loads[("tok", g)].wait()
@@ -474,7 +495,7 @@
                 onehots[s], own_half, preferred_element_type=f32
             ).astype(bf16)
         if g == 0:
-            pl.semaphore_wait(barrier, len(greet))
+            pl.semaphore_wait(barrier, jnp.where(is_end, places + 1, places + 2))
         for s in (1, 2):
             dispatch(s, g).start()
         rows[0, g * cp : (g + 1) * cp, :] = jnp.dot(
@@ -487,8 +508,10 @@
         dispatch(s, g).wait_recv()
         dispatch_forward(s, g, c).start()
 
-    def pair_copy(s):
-        return remote(pair_out.at[s], pair_in.at[s], pair_send.at[s], pair_recv.at[s], partner)
+    def pair_copy(s, h):
+        return remote(
+            pair_out.at[s, :, piece(h)], pair_in.at[s, :, piece(h)], pair_send.at[s, h], pair_recv.at[s, h], partner
+        )
 
     def moe(s):
         if s:
@@ -503,65 +526,74 @@
             return 0
 
         lax.fori_loop(0, blocks_f, gate_up, 0, unroll=True)
-        tile = min(256, hw)
-
-        def down(dst, side):
-            def body(j, _):
-                start = pl.multiple_of(side * hw + j * tile, LANES)
+        tile = min(256, pw)
+
+        def down(dst, side, h):
+            for j in range(pw // tile):
+                start = pl.multiple_of(side * hw + h * pw + j * tile, LANES)
                 acc = jnp.dot(hidden[...], wd[:, pl.ds(start, tile)], preferred_element_type=f32)
-                dst[s, :, pl.ds(pl.multiple_of(j * tile, LANES), tile)] = acc.astype(bf16)
-                return 0
-
-            lax.fori_loop(0, hw // tile, body, 0, unroll=True)
+                dst[s, :, h * pw + j * tile : h * pw + (j + 1) * tile] = acc.astype(bf16)
 
         if s == 0:
             loads["wd"].wait()
-        down(pair_out, oc)
-        pair_copy(s).start()
-        down(psum, c)
+        for h in range(pieces):
+            down(pair_out, oc, h)
+            pair_copy(s, h).start()
+        for h in range(pieces):
+            down(psum, c, h)
 
     far = (1 - z // 2) * 2
 
-    def end_copy(s):
-        return remote(psum.at[s, zrows(far, 2)], from_end.at[s], end_send.at[s], end_recv.at[s], mate_dev)
-
-    def mate_copy(s):
-        return remote(psum.at[s, zrows(mate)], from_mate.at[s], mate_send.at[s], mate_recv.at[s], mate_dev)
-
-    def inner_copy(s):
-        return remote(psum.at[s, zrows(far, 2)], from_inner.at[s], inner_send.at[s], inner_recv.at[s], across_dev)
-
-    def add_into(s, at, other):
-        psum[s, at, :] = (psum[s, at, :].astype(f32) + other.astype(f32)).astype(bf16)
+    def end_copy(s, h):
+        return remote(
+            psum.at[s, zrows(far, 2), piece(h)], from_end.at[s, :, piece(h)],
+            end_send.at[s, h], end_recv.at[s, h], mate_dev,
+        )
+
+    def mate_copy(s, h):
+        return remote(
+            psum.at[s, zrows(mate), piece(h)], from_mate.at[s, :, piece(h)],
+            mate_send.at[s, h], mate_recv.at[s, h], mate_dev,
+        )
+
+    def inner_copy(s, h):
+        return remote(
+            psum.at[s, zrows(far, 2), piece(h)], from_inner.at[s, :, piece(h)],
+            inner_send.at[s, h], inner_recv.at[s, h], across_dev,
+        )
+
+    def add_into(s, at, h, other):
+        psum[s, at, piece(h)] = (psum[s, at, piece(h)].astype(f32) + other.astype(f32)).astype(bf16)
 
     def stage1(s):
-        pair_copy(s).wait_recv()
+        for h in range(pieces):
+            pair_copy(s, h).wait_recv()
+
+            def body(k, _):
+                at = zrows(k)
+                add_into(s, at, h, pair_in[s, at, piece(h)])
+                return 0
+
+            lax.fori_loop(0, pairs, body, 0)
+
+            @pl.when(is_end)
+            def _():
+                end_copy(s, h).start()
+
+    def stage2(s, h):
+        end_copy(s, h).wait_recv()
 
         def body(k, _):
-            at = zrows(k)
-            add_into(s, at, pair_in[s, at, :])
+            add_into(s, zrows(far + k), h, from_end[s, zrows(k), piece(h)])
             return 0
 
-        lax.fori_loop(0, pairs, body, 0)
-
-        @pl.when(is_end)
-        def _():
-            end_copy(s).start()
-
-    def stage2(s):
-        end_copy(s).wait_recv()
-
-        def body(k, _):
-            add_into(s, zrows(far + k), from_end[s, zrows(k), :])
-            return 0
-
         lax.fori_loop(0, 2, body, 0)
-        inner_copy(s).start()
-
-    def stage3(s):
-        inner_copy(s).wait_recv()
-        add_into(s, zrows(mate), from_inner[s, zrows(mate % 2), :])
-        mate_copy(s).start()
+        inner_copy(s, h).start()
+
+    def stage3(s, h):
+        inner_copy(s, h).wait_recv()
+        add_into(s, zrows(mate), h, from_inner[s, zrows(mate % 2), piece(h)])
+        mate_copy(s, h).start()
 
     def inner(work):
         def run():
@@ -571,28 +603,22 @@
 
         return run
 
-    def result_copy(s):
+    def result_copy(s, h):
         return remote(
-            result_out.at[s], results.at[pl.ds(s * cp, cp)], ret_send.at[s - 1], ret_recv.at[s - 1], ep_peer[s]
-        )
-
-    def stage4(s, inside):
-        mate_copy(s).wait_recv()
-        total = psum[s, zrows(z), :].astype(f32) + from_mate[s].astype(f32)
-        here = slice(s * cp, (s + 1) * cp)
-
-        def put(value):
-            if s:
-                result_out[s] = value.astype(bf16)
-            else:
-                results[here, :] = value.astype(bf16)
-
+            result_out.at[s, :, piece(h)], results.at[pl.ds(s * cp, cp), piece(h)],
+            ret_send.at[s - 1, h], ret_recv.at[s - 1, h], ep_peer[s],
+        )
+
+    def stage4(s, h, inside):
+        mate_copy(s, h).wait_recv()
+        total = psum[s, zrows(z), piece(h)].astype(f32) + from_mate[s, :, piece(h)].astype(f32)
         if inside:
-            total = total + from_inner[s, zrows(z % 2), :].astype(f32)
-        put(total)
-
+            total = total + from_inner[s, zrows(z % 2), piece(h)].astype(f32)
         if s:
-            result_copy(s).start()
+            result_out[s, :, piece(h)] = total.astype(bf16)
+            result_copy(s, h).start()
+        else:
+            results[0:cp, piece(h)] = total.astype(bf16)
 
     def carry_copy(s):
         return remote(carries.at[0], carries.at[s], carry_send.at[s - 1], carry_recv.at[s - 1], ep_peer[s])
@@ -772,6 +798,12 @@
 
             own_copy(r, c).start()
 
+    def out_copy(r):
+        return pltpu.make_async_copy(out_buf.at[rows_of(r)], out_ref.at[rows_of(r)], out_sem.at[r])
+
+    def moe_copy():
+        return pltpu.make_async_copy(moe_buf, moe_ref, out_sem.at[ROW_CHUNKS])
+
     def project(j, inside, r):
         src = source(j, inside) if j else z
         if j:
@@ -785,7 +817,8 @@
         if j:
             part = part + out_acc[here, :]
         if j == last_z:
-            out_ref[here, :] = part.astype(bf16)
+            out_buf[here, :] = part.astype(bf16)
+            out_copy(r).start()
         else:
             out_acc[here, :] = part
 
@@ -817,7 +850,8 @@
             [jnp.where(picks[s], low[s : s + 1, :], 0.0).astype(bf16) for s in range(places)], axis=0
         )
         for s in range(1, places):
-            result_copy(s).wait_recv()
+            for h in range(pieces):
+                result_copy(s, h).wait_recv()
         total = lax.dot_general(coarse, results[...], TN, preferred_element_type=f32) + lax.dot_general(
             fine, results[...], TN, preferred_element_type=f32
         )
@@ -827,55 +861,91 @@
     def finish():
         moe_buf[:, half(c)] = combined[pl.ds(pl.multiple_of(c * sub, 16), sub), :]
         swap_in().wait_recv()
-        moe_ref[...] = moe_buf[...]
+        moe_copy().start()
 
     chunks = range(ROW_CHUNKS)
+    both = range(pieces)
     for j in range(blocks_f):
         loads[("wg", j)].wait()
         loads[("wu", j)].wait()
     moe(0)
-    for name in ("q", "f", "v"):
+    for name in ("q", "f", "v", "gap", "extra"):
         loads[name].wait()
 
-    def take(s):
-        for g in range(pairs):
+    def take(s, at):
+        for g in at:
             forward(s, g)
 
-    recurrence({1: lambda: stage1(0), 6: inner(lambda: stage2(0))})
-    take(1)
-    take(2)
+    def second(s):
+        for h in both:
+            stage2(s, h)
+
+    def third(s):
+        for h in both:
+            stage3(s, h)
+
+    def mates(s):
+        @pl.when(is_end)
+        def _():
+            for h in both:
+                mate_copy(s, h).start()
+
+    def starts(at):
+        @pl.when(is_end)
+        def _():
+            for r in at:
+                start_own(r)
+
+    recurrence(
+        {
+            1: lambda: (stage1(0), mates(0)),
+            3: lambda: (take(1, [0]), take(2, [0])),
+            5: lambda: (take(1, [1]), take(2, [1])),
+            6: inner(lambda: stage2(0, 0)),
+            7: lambda: (take(1, [2]), take(2, [2])),
+        }
+    )
+    take(1, [3])
+    take(2, [3])
+    inner(lambda: stage2(0, 1))()
     moe(1)
     loads["gate"].wait()
+    loads["head_gain"].wait()
     gated()
     stage1(1)
-    inner(lambda: stage3(0))()
     moe(2)
-    take(3)
+    inner(lambda: third(0))()
     stage1(2)
+    take(3, range(pairs))
     moe(3)
     loads["wo"].wait()
+    loads["weight"].wait()
     stage1(3)
 
     @pl.when(is_end)
     def _():
         for r in chunks:
             start_own(r)
-        for s in range(places):
-            mate_copy(s).start()
+        for s in range(1, places):
+            for h in both:
+                mate_copy(s, h).start()
         for r in chunks:
             project(0, False, r)
             ag_step(1, False, r)
-        stage4(0, False)
+        for h in both:
+            stage4(0, h, False)
         for r in chunks:
             ag_step(2, False, r)
             project(1, False, r)
-        stage4(1, False)
-        stage4(2, False)
+        for s in (1, 2):
+            for h in both:
+                stage4(s, h, False)
         for r in chunks:
             project(2, False, r)
         for r in (0, 1):
             ag_step(3, False, r)
-        stage4(3, False)
+        for h in both:
+            stage4(3, h, False)
         for r in (2, 3):
             ag_step(3, False, r)
         for r in chunks:
@@ -883,29 +953,35 @@
 
     @pl.when(is_inner)
     def _():
-        stage2(1)
+        second(1)
         for r in chunks:
             project(0, True, r)
             ag_step(1, True, r)
-        stage2(2)
-        stage3(1)
+        stage2(2, 0)
+        stage3(1, 0)
+        stage2(2, 1)
+        stage3(1, 1)
         for r in chunks:
             project(1, True, r)
-        stage2(3)
+        stage2(3, 0)
+        stage3(2, 0)
+        stage2(3, 1)
         ag_step(2, True, 0)
-        stage3(2)
+        stage3(2, 1)
         ag_step(2, True, 1)
         ag_step(3, True, 0)
+        stage3(3, 0)
         ag_step(2, True, 2)
         ag_step(3, True, 1)
-        stage3(3)
+        stage3(3, 1)
         ag_step(2, True, 3)
         ag_step(3, True, 2)
+        ag_step(3, True, 3)
         for r in chunks:
             project(2, True, r)
-        ag_step(3, True, 3)
         for s in range(places):
-            stage4(s, True)
+            for h in both:
+                stage4(s, h, True)
         for r in chunks:
             project(3, True, r)
 
@@ -917,21 +993,24 @@
             dispatch(s, g).wait_send()
             dispatch_forward(s, g, c).wait_send()
         carry_copy(s).wait_send()
-        result_copy(s).wait_send()
+        for h in both:
+            result_copy(s, h).wait_send()
     for s in range(places):
-        pair_copy(s).wait_send()
-        mate_copy(s).wait_send()
-
-        @pl.when(is_end)
-        def _():
-            end_copy(s).wait_send()
-
-        @pl.when(is_inner)
-        def _():
-            inner_copy(s).wait_send()
+        for h in both:
+            pair_copy(s, h).wait_send()
+            mate_copy(s, h).wait_send()
+
+            @pl.when(is_end)
+            def _():
+                end_copy(s, h).wait_send()
+
+            @pl.when(is_inner)
+            def _():
+                inner_copy(s, h).wait_send()
 
     for r in chunks:
         own_copy(r, c).wait_send()
+        out_copy(r).wait()
         for src in range(pairs):
 
             @pl.when((src <= z) & (z < last_z))
@@ -947,6 +1026,7 @@
                 ag_forward(src, r, c).wait_send()
 
     swap_copy().wait_send()
+    moe_copy().wait()
 
 
 def on_device(*arrays):
@@ -987,7 +1067,9 @@
     vmem = pl.BlockSpec(memory_space=pltpu.VMEM)
     anywhere = pl.BlockSpec(memory_space=pl.ANY)
     dma = pltpu.SemaphoreType.DMA
-    scratch = [
+    small = [index.T, weight.T, norm_gain.reshape(1, width), gap.reshape(1, keys), extra.T, head_gain.reshape(1, vals)]
+    scratch = [pltpu.VMEM(a.shape, a.dtype) for a in small]
+    scratch += [
         pltpu.VMEM((count, width), bf16),
         pltpu.VMEM((length, keys), bf16),
         pltpu.VMEM((length, keys), bf16),
@@ -1017,16 +1099,17 @@
         pltpu.VMEM((vals, keys), bf16),
         pltpu.VMEM((pairs, 2, length, vals), bf16),
         pltpu.VMEM((length, features), f32),
+        pltpu.VMEM((length, features), bf16),
     ]
-    n_loads = pairs + 2 * (hidden // LANES) + 6
+    n_loads = pairs + 2 * (hidden // LANES) + 12
     peers = places - 1
     sems = [dma((n_loads,))]
-    sems += [dma((peers, pairs))] * 4 + [dma((places,))] * 8 + [dma((peers,))] * 2 + [dma((1,))] * 2
-    sems += [dma((peers,))] * 2 + [dma((ROW_CHUNKS,))] * 2 + [dma((pairs, ROW_CHUNKS))] * 5
-    return pl.pallas_call(
+    sems += [dma((peers, pairs))] * 4 + [dma((places, 2))] * 8 + [dma((peers, 2))] * 2 + [dma((1,))] * 2
+    sems += [dma((peers,))] * 2 + [dma((ROW_CHUNKS,))] * 2 + [dma((pairs, ROW_CHUNKS))] * 5 + [dma((ROW_CHUNKS + 1,))]
+    outputs = pl.pallas_call(
         fused_kernel,
-        in_specs=[vmem] * 6 + [anywhere] * 9,
-        out_specs=[vmem, vmem],
+        in_specs=[anywhere] * 15,
+        out_specs=[anywhere, anywhere],
         out_shape=[
             jax.ShapeDtypeStruct((length, features), bf16),
             jax.ShapeDtypeStruct((sub, width), bf16),
@@ -1037,9 +1120,43 @@
         ),
         name="fused_layer",
     )(
-        index.T, weight.T, norm_gain.reshape(1, width), gap.reshape(1, keys), extra.T,
-        head_gain.reshape(1, vals), tokens, query, forget, values, gate, out_weight,
+        *small, tokens, query, forget, values, gate, out_weight,
         gate_weight, up_weight, down_weight,
+    )
+    parts = [(0, r * length // 4, length // 4) for r in range(4)] + [(1, 0, sub)]
+
+    def deliver(first, second, out_first, out_second, buf, small_buf, sem_in, sem_out):
+        sources, targets, bufs = (first, second), (out_first, out_second), (buf, small_buf)
+        into = [
+            pltpu.make_async_copy(sources[w].at[pl.ds(a, n)], bufs[w].at[pl.ds(a, n)], sem_in.at[i])
+            for i, (w, a, n) in enumerate(parts)
+        ]
+        outof = [
+            pltpu.make_async_copy(bufs[w].at[pl.ds(a, n)], targets[w].at[pl.ds(a, n)], sem_out.at[i])
+            for i, (w, a, n) in enumerate(parts)
+        ]
+        for copy in into:
+            copy.start()
+        for i, copy in enumerate(into):
+            copy.wait()
+            outof[i].start()
+        for copy in outof:
+            copy.wait()
+
+    return tuple(
+        pl.pallas_call(
+            deliver,
+            in_specs=[anywhere] * 2,
+            out_specs=[anywhere] * 2,
+            out_shape=[jax.ShapeDtypeStruct((length, features), bf16), jax.ShapeDtypeStruct((sub, width), bf16)],
+            scratch_shapes=[
+                pltpu.VMEM((length, features), bf16),
+                pltpu.VMEM((sub, width), bf16),
+                dma((len(parts),)),
+                dma((len(parts),)),
+            ],
+            name="deliver",
+        )(*outputs)
     )
 
 

time: 106 us -> 104 us (0.981)
  local copies, waits for them, and re-layouts: 3.93 us -> 0 us
  Pallas kernels: 101 us -> 103 us
    unnamed x2 -> x0, local copies, waits for them, and re-layouts: 3.93 us -> none
    pallas_call x1 -> x2, Pallas kernels: 101 us -> 103 us  [the longest x1 101 us: on_device(): pl.pallas_call(fused_kernel, in_specs=[anywhere] * 15, out_specs=[anywher...]
where the time goes in v3:
time: 104 us
  Pallas kernels  103 us (99%)
    pallas_call x1, Pallas kernels, on_device(): pl.pallas_call(fused_kernel, in_specs=[anywhere] * 15, out_specs=[anywher...  101 us
    pallas_call x1, Pallas kernels, on_device(): pl.pallas_call(deliver, in_specs=[anywhere] * 2, out_specs=[anywhere] * 2...  2.08 us

profile of v3, /device:TPU:0, one launch (start us, length us, event | category | flops | bytes accessed | tf_op | source)
XLA Modules:
  0.0 104.1 jit_solution(10936002010524646966)
XLA Ops:
  0.6 101.1 %fused_layer.1 = (bf16[2048,256]{1,0:T(8,128)(2,1)}, bf16[64,2048]{1,0:T(8,128)(2,1)}) custom-call(s32[2,512]{1,0:T(2,128)} %bitcast.8, f32[2,512]{1,0:T(2,128)} %bitcast.9, f32[1,2048]{1,0:T(1,128)} %bitcast.7, f32[1,256]{1,0:T(1,128)} %bitcast.10, f32[2,2048]{1,0:T(2,128)} %bitcast.6, f32[1,128]{1,0:T(1,128)} %bitcast.11, bf16[512,2048]{1,0:T(8,128)(2,1)} %tok_hbm.1, ...), custom_call_target="tpu_custom_call" | custom-call | tf_op jit(solution)/shard_map/fused_layer/pallas_call | solution.py:1109
  101.8 2.1 %deliver.1 = (bf16[2048,256]{1,0:T(8,128)(2,1)}, bf16[64,2048]{1,0:T(8,128)(2,1)}) custom-call(bf16[2048,256]{1,0:T(8,128)(2,1)} %get-tuple-element.4.first, bf16[64,2048]{1,0:T(8,128)(2,1)} %get-tuple-element.5.second), custom_call_target="tpu_custom_call" | custom-call | tf_op jit(solution)/shard_map/deliver/pallas_call | solution.py:1147

commit v4 on v3

--- a/solution.py
+++ b/solution.py
@@ -909,11 +909,11 @@
     take(2, [3])
     inner(lambda: stage2(0, 1))()
     moe(1)
+    stage1(1)
+    moe(2)
     loads["gate"].wait()
     loads["head_gain"].wait()
     gated()
-    stage1(1)
-    moe(2)
     inner(lambda: third(0))()
     stage1(2)
     take(3, range(pairs))

time: 104 us -> 101 us (0.971)
  Pallas kernels: 103 us -> 99.5 us
    pallas_call x1, Pallas kernels: 101 us -> 97.4 us  [on_device(): pl.pallas_call(fused_kernel, in_specs=[anywhere] * 15, out_specs=[anywher...]
where the time goes in v4:
time: 101 us; the launch traced here: 100 us
  Pallas kernels  99.5 us (99%)
    pallas_call x1, Pallas kernels, on_device(): pl.pallas_call(fused_kernel, in_specs=[anywhere] * 15, out_specs=[anywher...  97.4 us
    pallas_call x1, Pallas kernels, on_device(): pl.pallas_call(deliver, in_specs=[anywhere] * 2, out_specs=[anywhere] * 2...  2.08 us

profile of v4, /device:TPU:0, one launch (start us, length us, event | category | flops | bytes accessed | tf_op | source)
XLA Modules:
  0.0 100.3 jit_solution(4979266232884290818)
XLA Ops:
  0.6 97.4 %fused_layer.1 = (bf16[2048,256]{1,0:T(8,128)(2,1)}, bf16[64,2048]{1,0:T(8,128)(2,1)}) custom-call(s32[2,512]{1,0:T(2,128)} %bitcast.8, f32[2,512]{1,0:T(2,128)} %bitcast.9, f32[1,2048]{1,0:T(1,128)} %bitcast.7, f32[1,256]{1,0:T(1,128)} %bitcast.10, f32[2,2048]{1,0:T(2,128)} %bitcast.6, f32[1,128]{1,0:T(1,128)} %bitcast.11, bf16[512,2048]{1,0:T(8,128)(2,1)} %tok_hbm.1, ...), custom_call_target="tpu_custom_call" | custom-call | tf_op jit(solution)/shard_map/fused_layer/pallas_call | solution.py:1109
  98.1 2.1 %deliver.1 = (bf16[2048,256]{1,0:T(8,128)(2,1)}, bf16[64,2048]{1,0:T(8,128)(2,1)}) custom-call(bf16[2048,256]{1,0:T(8,128)(2,1)} %get-tuple-element.4.first, bf16[64,2048]{1,0:T(8,128)(2,1)} %get-tuple-element.5.second), custom_call_target="tpu_custom_call" | custom-call | tf_op jit(solution)/shard_map/deliver/pallas_call | solution.py:1147
